TPU v7x, 256 devices: a whole 4x4x8 slice. The times are simulated.
256 devices in a mesh: fs: 64 (over z, y, core), tp: 4 (over x).
Axes of the slice: x: 4, y: 4, z: 8, core: 2. Of those that a mesh axis runs over, the one named last changes fastest.
Arguments:
- later_gate: bfloat16 [40960, 5632], P('fs', 'tp'), may hold values from -6 to 6
- later_up: bfloat16 [40960, 5632], P('fs', 'tp'), may hold values from -6 to 6
- early_gate: bfloat16 [40960, 5632], P('fs', 'tp'), may hold values from -6 to 6
- early_up: bfloat16 [40960, 5632], P('fs', 'tp'), may hold values from -6 to 6
- early_cotangent: bfloat16 [40960, 2048], P(('fs', 'tp')), may hold values from -24 to 24
- down_weight: bfloat16 [5632, 2048], P('tp', 'fs'), may hold values from -0.078125 to 0.078125
- grad_running: float32 [5632, 2048], P('tp', 'fs'), may hold values from -640 to 640
Outputs:
- mixed: bfloat16 [40960, 2048], P(('fs', 'tp'))
- gate_grad: bfloat16 [40960, 5632], P('fs', 'tp')
- up_grad: bfloat16 [40960, 5632], P('fs', 'tp')
- grad_total: float32 [5632, 2048], P('tp', 'fs')
All inputs are finite; a program needn't handle non-finite values.
Results may differ from a plain program's by a relative error of at most 0.009.
Values may be sent and summed in bfloat16 or wider, within the bound.
No kernel may reach another device: no remote copies, remote signals or barrier semaphores. Data moves between devices by JAX's collectives and lax.ppermute only.
A program may use at most 128 MiB of HBM per device.

v0:
```python
import jax
import jax.numpy as jnp
from jax import lax
from jax.sharding import PartitionSpec as P


def laid_out(tiles, dim):
    dims = list(tiles.shape[1:])
    dims[dim] *= tiles.shape[0]
    return jnp.moveaxis(tiles, 0, dim).reshape(dims)


def copy_for_each(x, axis):
    size = lax.axis_size(axis)
    return lax.all_to_all(jnp.broadcast_to(x[None], (size, *x.shape)), axis, 0, 0, tiled=True)


def gather_directly(x, axis, dim):
    return laid_out(copy_for_each(x, axis), dim)


def cut_along(x, dim, size):
    before, after = (x.shape[:dim], x.shape[dim + 1 :])
    return jnp.moveaxis(x.reshape(*before, size, -1, *after), dim, 0)


def sent_and_summed(x, axis, dim):
    tiles = cut_along(x, dim, lax.axis_size(axis))
    arrived = lax.all_to_all(tiles, axis, split_axis=0, concat_axis=0, tiled=True)
    return arrived.astype(jnp.float32).sum(axis=0)


def on_device(
    later_gate, later_up, early_gate, early_up, early_cotangent, down_weight, grad_running
):
    later_hidden = (
        jax.nn.silu(later_gate.astype(jnp.float32)) * later_up.astype(jnp.float32)
    ).astype(jnp.bfloat16)
    gate_value = early_gate.astype(jnp.float32)
    up_value = early_up.astype(jnp.float32)
    sigma = jax.nn.sigmoid(gate_value)
    early_hidden = (gate_value * sigma * up_value).astype(jnp.bfloat16)
    cot_rows = gather_directly(early_cotangent, "tp", 0)
    whole = lax.all_gather(down_weight, "fs", axis=1, tiled=True)
    mixed = sent_and_summed(
        jnp.dot(later_hidden, whole, preferred_element_type=jnp.float32).astype(jnp.bfloat16),
        "tp",
        0,
    ).astype(jnp.bfloat16)
    hidden_cot = lax.dot_general(
        cot_rows, whole, (((1,), (1,)), ((), ())), preferred_element_type=jnp.float32
    )
    gate_grad = (hidden_cot * up_value * sigma * (1.0 + gate_value * (1.0 - sigma))).astype(
        jnp.bfloat16
    )
    up_grad = (hidden_cot * gate_value * sigma).astype(jnp.bfloat16)
    summed = lax.psum_scatter(
        lax.dot_general(
            cot_rows, early_hidden, (((0,), (0,)), ((), ())), preferred_element_type=jnp.float32
        ),
        "fs",
        scatter_dimension=0,
        tiled=True,
    )
    grad_total = grad_running + summed.T
    return (mixed, gate_grad, up_grad, grad_total)


def solution(mesh):
    placed = (
        P("fs", "tp"),
        P("fs", "tp"),
        P("fs", "tp"),
        P("fs", "tp"),
        P(("fs", "tp"), None),
        P("tp", "fs"),
        P("tp", "fs"),
    )
    return jax.shard_map(
        on_device,
        mesh=mesh,
        in_specs=placed,
        out_specs=(P(("fs", "tp"), None), P("fs", "tp"), P("fs", "tp"), P("tp", "fs")),
        check_vma=False,
    )
```

profile of v0, /device:TPU:2, one launch (start us, length us, event | category | flops | bytes accessed | tf_op | source)
XLA Modules:
  0.0 263.2 jit_solution(15338845092056595441)
XLA Ops:
  7.2 0.0 all-gather.2.cloned.1.call-start
  7.2 0.7 all-gather.2.cloned.1.call-update
  7.9 0.0 copy-start.3
  7.9 0.0 reduce-scatter.4.cloned.1.call-start
  8.0 0.0 copy-start.4
  8.0 1.5 broadcast_in_dim.2
  9.5 35.1 %all_to_all.10 = bf16[4,160,2048]{2,1,0:T(8,128)(2,1)S(1)} all-to-all(bf16[4,160,2048]{2,1,0:T(8,128)(2,1)S(1)} %broadcast_in_dim.2), channel_id=1, replica_groups=mesh['fs'=64,'tp'=4] {'tp'}, dimensions={0} | all-to-all | bytes 5242880 | tf_op jit(solution)/shard_map/all_to_all | solution.py:15
  44.6 0.0 copy-start
  44.6 1.5 copy-done
  46.1 0.0 copy-done.3
  46.2 0.0 copy-done.4
  46.2 7.9 %convolution_bitcast_fusion = f32[2048,1408]{0,1:T(8,128)} fusion(bf16[640,2048]{1,0:T(8,128)(2,1)S(1)} %bitcast.11, bf16[640,1408]{1,0:T(8,128)(2,1)S(1)} %copy-done.4, bf16[640,1408]{1,0:T(8,128)(2,1)S(1)} %copy-done.3), kind=kOutput, calls=%fused_computation | convolution fusion | flops 3698196480 | bytes 17760256 | tf_op jit(solution)/shard_map/dot_general | solution.py:58
  54.0 12.0 %copy.15 = f32[2048,1408]{1,0:T(8,128)} copy(f32[2048,1408]{0,1:T(8,128)} %convolution_bitcast_fusion) | data formatting | bytes 23068672
  66.1 0.0 copy-start.2
  66.1 0.0 reduce-scatter.4.cloned.1.call-update
  66.1 27.7 %all-gather.2.cloned.1.call-done = bf16[1408,2048]{0,1:T(8,128)(2,1)} async-done(((bf16[1408,32]{0,1:T(8,128)(2,1)}), bf16[1408,2048]{0,1:T(8,128)(2,1)}) %all-gather.2.cloned.1.call-update) | async-done | bytes 5767184 | tf_op jit(solution)/shard_map/all_gather | solution.py:44
  93.8 0.0 copy-done.2
  93.8 9.2 %convolution_convert_fusion = bf16[640,2048]{1,0:T(8,128)(2,1)} fusion(bf16[1408,2048]{0,1:T(8,128)(2,1)} %all-gather.2.cloned.1.call-done, bf16[640,1408]{1,0:T(8,128)(2,1)S(1)} %copy-done.2, bf16[640,1408]{1,0:T(8,128)(2,1)} %param.7), kind=kOutput, calls=%fused_computation.24 | convolution fusion | flops 3699507200 | bytes 11993088 | tf_op jit(solution)/shard_map/dot_general | solution.py:46
  102.9 0.0 copy-start.1
  102.9 4.9 %all-to-all-start = ((bf16[4,160,2048]{2,1,0:T(8,128)(2,1)}), bf16[4,160,2048]{2,1,0:T(8,128)(2,1)S(1)}, u32[]{:S(2)}, u32[]{:S(2)}) async-start(bf16[4,160,2048]{2,1,0:T(8,128)(2,1)} %bitcast.13), calls=%async_computation | async-start | bytes 5242880 | tf_op jit(solution)/shard_map/all_to_all | solution.py:29
  107.9 0.0 copy-done.1
  107.9 0.3 copy.13
  108.1 11.9 %fusion.13 = (bf16[640,1408]{1,0:T(8,128)(2,1)}, bf16[640,1408]{1,0:T(8,128)(2,1)}) fusion(bf16[640,1408]{1,0:T(8,128)(2,1)} %param.9, bf16[640,1408]{1,0:T(8,128)(2,1)} %param.10, bf16[640,2048]{1,0:T(8,128)(2,1)} %bitcast.12, bf16[1408,2048]{0,1:T(8,128)(2,1)} %all-gather.2.cloned.1.call-done), kind=kOutput, calls=%fused_computation.22 | convolution fusion | flops 3704504320 | bytes 15597568 | tf_op jit(solution)/shard_map/dot_general | solution.py:50
  120.1 18.7 %all-to-all-done = bf16[4,160,2048]{2,1,0:T(8,128)(2,1)S(1)} async-done(((bf16[4,160,2048]{2,1,0:T(8,128)(2,1)}), bf16[4,160,2048]{2,1,0:T(8,128)(2,1)S(1)}, u32[]{:S(2)}, u32[]{:S(2)}) %all-to-all-start) | async-done | bytes 2621472 | tf_op jit(solution)/shard_map/all_to_all | solution.py:29
  138.8 1.5 reduce_sum.12
  140.3 113.9 %reduce-scatter.4.cloned.1.call-done = f32[32,1408]{1,0:T(8,128)} async-done(((f32[2048,1408]{1,0:T(8,128)}), f32[32,1408]{1,0:T(8,128)}) %reduce-scatter.4.cloned.1.call-update) | async-done | bytes 180240
  254.2 1.2 copy.16
  255.4 0.1 bitcast_add_fusion
  255.5 0.9 copy.14
Async XLA Ops:
  7.2 86.6 %all-gather.2.cloned.1.call-start = ((), (), s32[]{:S(2)}) async-start(), calls=%async_computation.3 | async-start | bytes 5857280 | tf_op jit(solution)/shard_map/all_gather | solution.py:44
  7.9 38.3 %copy-start.3 = (bf16[640,1408]{1,0:T(8,128)(2,1)S(1)}, bf16[640,1408]{1,0:T(8,128)(2,1)}, u32[]{:S(2)}) copy-start(bf16[640,1408]{1,0:T(8,128)(2,1)} %param.9) | copy-start | bytes 5406724
  7.9 246.3 %reduce-scatter.4.cloned.1.call-start = ((), (), s32[]{:S(2)}) async-start(), calls=%async_computation.4 | async-start | bytes 11714560
  8.0 38.2 %copy-start.4 = (bf16[640,1408]{1,0:T(8,128)(2,1)S(1)}, bf16[640,1408]{1,0:T(8,128)(2,1)}, u32[]{:S(2)}) copy-start(bf16[640,1408]{1,0:T(8,128)(2,1)} %param.10) | copy-start | bytes 5406724
  44.6 1.5 copy-start
  66.1 27.7 %copy-start.2 = (bf16[640,1408]{1,0:T(8,128)(2,1)S(1)}, bf16[640,1408]{1,0:T(8,128)(2,1)}, u32[]{:S(2)}) copy-start(bf16[640,1408]{1,0:T(8,128)(2,1)} %param.8) | copy-start | bytes 5406724
  102.9 4.9 %copy-start.1 = (f32[1408,32]{0,1:T(8,128)S(1)}, f32[1408,32]{0,1:T(8,128)}, u32[]{:S(2)}) copy-start(f32[1408,32]{0,1:T(8,128)} %param.13) | copy-start | bytes 540676
  102.9 35.8 %all-to-all-start = ((bf16[4,160,2048]{2,1,0:T(8,128)(2,1)}), bf16[4,160,2048]{2,1,0:T(8,128)(2,1)S(1)}, u32[]{:S(2)}, u32[]{:S(2)}) async-start(bf16[4,160,2048]{2,1,0:T(8,128)(2,1)} %bitcast.13), calls=%async_computation | async-start | bytes 5242880 | tf_op jit(solution)/shard_map/all_to_all | solution.py:29
Sparse Core Ops, SparseCore 0:
  10.7 83.0 all-gather.1
  98.0 156.0 reduce-scatter.3
where the time goes:
time: 264 us; the launch traced here: 263 us
  waiting for transfers between devices  161 us (61%)
  blocking collectives  35.1 us (13%)
  matrix products  29 us (11%)
  local copies, waits for them, and re-layouts  17.5 us (7%)
  between operations  14.1 us (5%)
  starting transfers between devices  5.01 us (2%)
    unnamed x3, waiting for transfers between devices  115 us
    all_to_all x1, blocking collectives, copy_for_each(): lax.all_to_all(jnp.broadcast_to(x[None], (size, *x.shape)), axis, 0, 0, t...  35.1 us
    all_gather x1, waiting for transfers between devices, on_device(): whole = lax.all_gather(down_weight, 'fs', axis=1, tiled=True)  27.7 us
    all_to_all x1, waiting for transfers between devices, sent_and_summed(): lax.all_to_all(tiles, axis, split_axis=0, concat_axis=0, tiled=True)  18.7 us
    unnamed x14, local copies, waits for them, and re-layouts  15.9 us
    dot_general x1, matrix products, on_device(): lax.dot_general(cot_rows, whole, (((1,), (1,)), ((), ())), preferred_elem...  11.9 us
    dot_general x1, matrix products, on_device(): jnp.dot(later_hidden, whole, preferred_element_type=jnp.float32)  9.17 us
    dot_general x1, matrix products, on_device(): lax.dot_general(cot_rows, early_hidden, (((0,), (0,)), ((), ())), preferr...  7.87 us
  transfers between devices with their start and end apart: 3, of which 3 were waited for; matrix products, arithmetic and copies ran while one was open for 17% of the time, Pallas kernels for 0%

commit v1 on v0

v1 whole, which is shorter than its diff:
```python
import jax
import jax.numpy as jnp
from jax import lax
from jax.experimental import pallas as pl
from jax.experimental.pallas import tpu as pltpu
from jax.sharding import PartitionSpec as P


BF = jnp.bfloat16
F32 = jnp.float32
NZ, NY, NC, NX = 8, 4, 2, 4


def fs_id(z, y, c):
    return (z % NZ) * (NY * NC) + (y % NY) * NC + c % NC


def grad_term(where, cot, hidden):
    n, d = cot.shape
    ff = hidden.shape[1]
    w = d // (NZ * NY * NC)
    zs = 2
    tile = zs * NY * NC * w

    def body(where, cot, hidden, give, keep):
        y, c = where[1], where[2]
        tile_term = lax.dot_general(
            cot[...], hidden[...], (((0,), (0,)), ((), ())), preferred_element_type=F32
        ).reshape(zs, NY, NC, w, ff)
        early = pl.program_id(0) * zs < NZ // 2
        for i in range(NY):
            yr = lax.rem(i - y + NY, NY)
            first = jnp.where(yr == 1, 2, jnp.where(yr == 2, 0, 1))
            last = jnp.where(yr == 1, 0, jnp.where(yr == 2, 1, 2))
            slot = jnp.where(yr == 0, 3, jnp.where(early, first, last))
            for j in range(zs):
                zero, one = tile_term[j, i, 0], tile_term[j, i, 1]
                keep[slot, j] = jnp.where(c == 0, zero, one).astype(BF)
                give[slot, j] = jnp.where(c == 0, one, zero).astype(BF)

    def out_index(i, where):
        return (0, i, 0, 0)

    return pl.pallas_call(
        body,
        grid_spec=pltpu.PrefetchScalarGridSpec(
            num_scalar_prefetch=1,
            grid=(NZ // zs,),
            in_specs=[
                pl.BlockSpec((n, tile), lambda i, where: (0, i)),
                pl.BlockSpec((n, ff), lambda i, where: (0, 0)),
            ],
            out_specs=[
                pl.BlockSpec((NY, zs, w, ff), out_index),
                pl.BlockSpec((NY, zs, w, ff), out_index),
            ],
        ),
        out_shape=[
            jax.ShapeDtypeStruct((NY, NZ, w, ff), BF),
            jax.ShapeDtypeStruct((NY, NZ, w, ff), BF),
        ],
        compiler_params=pltpu.CompilerParams(dimension_semantics=("arbitrary",)),
        cost_estimate=pl.CostEstimate(
            flops=2 * n * d * ff, bytes_accessed=12 * 1024 * 1024, transcendentals=0
        ),
        name="grad_term",
    )(where, cot, hidden)


def partial_products(where, hidden, own, other):
    parts, rows, ff = hidden.shape
    count = len(own)
    w = own[0][0].shape[1]
    tile = NY * NC * w
    d = count * tile
    pieces, places = [], []
    for cr, blocks in enumerate((own, other)):
        for zr, block in enumerate(blocks):
            yr = 0
            for piece in block:
                for j in range(piece.shape[0]):
                    places.append((zr, cr, yr, len(pieces), j))
                    yr += 1
                pieces.append(piece)
    n = len(pieces)

    def body(where, hidden, *refs):
        blocks = refs[:n]
        outs, whole = refs[n : n + parts], refs[n + parts]
        ordered, weight, sems = refs[n + parts + 1 :]
        step = pl.program_id(0)
        y, c, t = where[1], where[2], where[3]

        def copies(at):
            return [
                pltpu.make_async_copy(
                    blocks[i].at[j],
                    weight.at[zr, lax.rem(y + yr, NY), lax.rem(c + cr, NC)],
                    sems.at[zr, cr, yr],
                )
                for zr, cr, yr, i, j in places
                if zr == at
            ]

        @pl.when(step == 0)
        def _():
            for zr in range(count):
                for copy in copies(zr):
                    copy.start()
            for i in range(parts):
                ordered[pl.ds(i * rows, rows), :] = hidden[lax.rem(t + i, parts)]

        for zr in range(count):

            @pl.when(step == zr)
            def _(zr=zr):
                for copy in copies(zr):
                    copy.wait()

        part = lax.dot_general(
            ordered[...],
            weight[step].reshape(tile, ff),
            (((1,), (1,)), ((), ())),
            preferred_element_type=F32,
        ).astype(BF)
        for i in range(parts):
            outs[i][...] = part[i * rows : (i + 1) * rows]
        whole[0] = weight[step]

    def at(i, where):
        return lax.rem(i + where[0], NZ)

    return pl.pallas_call(
        body,
        grid_spec=pltpu.PrefetchScalarGridSpec(
            num_scalar_prefetch=1,
            grid=(count,),
            in_specs=[pl.BlockSpec((parts, rows, ff), lambda i, where: (0, 0, 0))]
            + [pl.BlockSpec(memory_space=pltpu.HBM)] * n,
            out_specs=[pl.BlockSpec((rows, tile), lambda i, where: (0, at(i, where)))]
            * parts
            + [
                pl.BlockSpec(
                    (1, NY, NC, w, ff), lambda i, where: (at(i, where), 0, 0, 0, 0)
                )
            ],
            scratch_shapes=[
                pltpu.VMEM((parts * rows, ff), BF),
                pltpu.VMEM((count, NY, NC, w, ff), BF),
                pltpu.SemaphoreType.DMA((count, NC, NY)),
            ],
        ),
        out_shape=[jax.ShapeDtypeStruct((rows, d), BF)] * parts
        + [jax.ShapeDtypeStruct((count, NY, NC, w, ff), BF)],
        compiler_params=pltpu.CompilerParams(dimension_semantics=("arbitrary",)),
        cost_estimate=pl.CostEstimate(
            flops=2 * parts * rows * d * ff,
            bytes_accessed=16 * 1024 * 1024,
            transcendentals=0,
        ),
        name="partial_products",
    )(where, hidden, *pieces)


def pick(x, i, n):
    return lax.dynamic_index_in_dim(x, i % n, 0, keepdims=False)


def shift(x, dz=0, dy=0, dc=0):
    perm = [
        (fs_id(z, y, c), fs_id(z + dz, y + dy, c + dc))
        for z in range(NZ)
        for y in range(NY)
        for c in range(NC)
    ]
    return lax.ppermute(x, "fs", perm)


def shift_x(x, d):
    return lax.ppermute(x, "tp", [(i, (i + d) % NX) for i in range(NX)])


def step(
    later_gate, later_up, early_gate, early_up, early_cotangent, down_weight, grad_running
):
    k = lax.axis_index("fs")
    t = lax.axis_index("tp")
    where = jnp.stack([k // (NY * NC), (k // NC) % NY, k % NC, t]).astype(jnp.int32)
    rows, d = early_cotangent.shape
    ff, _ = down_weight.shape

    h = rows // 2
    cot = early_cotangent
    from_m = shift_x(cot, 1)
    from_p = shift_x(cot, -1)
    far_top = shift_x(from_m[:h], 1)
    far_bot = shift_x(from_p[h:], -1)
    cot_rows = jnp.zeros((NX, rows, d), BF)

    def put(buf, x, i, j=0):
        return lax.dynamic_update_slice(buf, x[None], ((t + i) % NX, j, 0))

    cot_rows = put(cot_rows, cot, 0)
    cot_rows = put(cot_rows, from_p, 1)
    cot_rows = put(cot_rows, from_m, 3)
    cot_rows = put(cot_rows, far_top, 2)
    cot_rows = put(cot_rows, far_bot, 2, h).reshape(NX * rows, d)

    later_hidden = (
        jax.nn.silu(later_gate.astype(F32)) * later_up.astype(F32)
    ).astype(BF)
    gate_value = early_gate.astype(F32)
    up_value = early_up.astype(F32)
    sigma = jax.nn.sigmoid(gate_value)
    early = lax.optimization_barrier((early_gate, early_up))
    early_hidden = (jax.nn.silu(early[0].astype(F32)) * early[1].astype(F32)).astype(BF)

    w0 = down_weight.T
    wy = jnp.stack([w0, shift(w0, dy=-1), shift(w0, dy=2), shift(w0, dy=1)])
    up1, dn1 = shift(wy, dz=1), shift(wy, dz=-1)
    c0 = shift(wy, dc=1)
    up2, dn2 = shift(up1, dz=1), shift(dn1, dz=-1)
    c1, c7 = shift(dn1, dc=1), shift(up1, dc=1)

    give, keep = grad_term(where, cot_rows, early_hidden)
    came = shift(give, dc=1)
    up_y, dn_y, fwd_y, own_y = (
        keep[i].astype(F32) + came[i].astype(F32) for i in range(NY)
    )

    up3, dn3 = shift(up2, dz=1), shift(dn2, dz=-1)
    c2, c6 = shift(dn2, dc=1), shift(up2, dc=1)

    q = NZ // 2
    up = shift(up_y.astype(BF), dy=1)
    dn = shift(dn_y.astype(BF), dy=-1)

    far = shift(up3, dz=1)
    c3, c5 = shift(dn3, dc=1), shift(up3, dc=1)
    c4 = shift(far, dc=1)
    own = [[wy], [dn1], [dn2], [dn3], [far], [up3], [up2], [up1]]
    other = [[c0], [c1], [c2], [c3], [c4], [c5], [c6], [c7]]

    up2y = shift((fwd_y[:q] + up[:q].astype(F32)).astype(BF), dy=1)
    dn2y = shift((fwd_y[q:] + dn[q:].astype(F32)).astype(BF), dy=-1)
    first = own_y[:q] + dn[:q].astype(F32) + up2y.astype(F32)
    last = own_y[q:] + up[q:].astype(F32) + dn2y.astype(F32)
    reduced = jnp.concatenate([first, last]).astype(BF)
    summed = pick(reduced, where[0], NZ).astype(F32)
    for i in (4, 3, 5, 2, 6, 1, 7):
        block = pick(reduced, where[0] + i, NZ)
        summed = summed + shift(block, dz=i).astype(F32)
    grad_total = grad_running + summed.T

    p0, p1, p2, p3, whole = partial_products(
        where, later_hidden.reshape(NX, rows, ff), own, other
    )
    total = p0.astype(F32)
    for i, p in ((2, p2), (1, p1), (3, p3)):
        total = total + shift_x(p, i).astype(F32)
    mixed = total.astype(BF)

    hidden_cot = jnp.dot(
        cot_rows, whole.reshape(d, ff), preferred_element_type=F32
    )
    gate_grad = (
        hidden_cot * up_value * sigma * (1.0 + gate_value * (1.0 - sigma))
    ).astype(BF)
    up_grad = (hidden_cot * gate_value * sigma).astype(BF)
    return (mixed, gate_grad, up_grad, grad_total)


def solution(mesh):
    placed = (
        P("fs", "tp"),
        P("fs", "tp"),
        P("fs", "tp"),
        P("fs", "tp"),
        P(("fs", "tp"), None),
        P("tp", "fs"),
        P("tp", "fs"),
    )
    return jax.shard_map(
        step,
        mesh=mesh,
        in_specs=placed,
        out_specs=(P(("fs", "tp"), None), P("fs", "tp"), P("fs", "tp"), P("tp", "fs")),
        check_vma=False,
    )
```

time: 264 us -> 172 us (0.65)
  the two profiles are of different devices: /device:TPU:2 before, /device:TPU:6 now
where the time goes in v1:
time: 172 us; the launch traced here: 171 us
  waiting for transfers between devices  68.4 us (40%)
  starting transfers between devices  50.2 us (29%)
  Pallas kernels  21.1 us (12%)
  other arithmetic  15.3 us (9%)
  matrix products  9.23 us (5%)
  local copies, waits for them, and re-layouts  6.16 us (4%)
    ppermute x30, starting transfers between devices, shift(): return lax.ppermute(x, 'fs', perm)  39.8 us
    ppermute x30, waiting for transfers between devices, shift(): return lax.ppermute(x, 'fs', perm)  37.5 us
    ppermute x7, waiting for transfers between devices, shift_x(): return lax.ppermute(x, 'tp', [(i, (i + d) % NX) for i in range(NX)])  30.9 us
    pallas_call x1, Pallas kernels, partial_products(): pl.pallas_call(body, grid_spec=pltpu.PrefetchScalarGridSpec(num_scalar_pr...  11.6 us
    ppermute x7, starting transfers between devices, shift_x(): return lax.ppermute(x, 'tp', [(i, (i + d) % NX) for i in range(NX)])  10.4 us
    pallas_call x1, Pallas kernels, grad_term(): pl.pallas_call(body, grid_spec=pltpu.PrefetchScalarGridSpec(num_scalar_pr...  9.52 us
    dot_general x1, matrix products, step(): jnp.dot(cot_rows, whole.reshape(d, ff), preferred_element_type=F32)  9.23 us
    convert_element_type x1, other arithmetic, step(): (jax.nn.silu(early[0].astype(F32)) * early[1].astype(F32)).astype(BF)  4.35 us
  transfers between devices with their start and end apart: 37, of which 14 were waited for; matrix products, arithmetic and copies ran while one was open for 16% of the time, Pallas kernels for 7%

profile of v1, /device:TPU:6, one launch (start us, length us, event | category | flops | bytes accessed | tf_op | source)
XLA Modules:
  0.0 171.3 jit_solution(12713793269667522787)
XLA Ops:
  0.6 0.9 collective-permute-start.21
  1.5 2.4 %collective-permute-start.22 = (bf16[160,2048]{1,0:T(8,128)(2,1)}, bf16[160,2048]{1,0:T(8,128)(2,1)}, u32[]{:S(2)}, u32[]{:S(2)}) collective-permute-start(bf16[160,2048]{1,0:T(8,128)(2,1)} %param.11), channel_id=1, source_target_pairs={{0,1},{1,2},{2,3},{3,0},{4,5},{5,6},{6,7},{7,4},{8,9},{9,10},{10,1... | collective-permute-start | bytes 1966088 | tf_op jit(solution)/shard_map/ppermute | solution.py:180
  3.9 4.3 %fusion.16.hidden = bf16[640,1408]{1,0:T(8,128)(2,1)} fusion(bf16[640,1408]{1,0:T(8,128)(2,1)} %param.10, bf16[640,1408]{1,0:T(8,128)(2,1)} %param.9), kind=kLoop, calls=%fused_computation.23 | loop fusion | flops 7208960 | bytes 5406720 | tf_op jit(solution)/shard_map/convert_element_type | solution.py:216
  8.3 0.7 pad_add_fusion.where
  8.9 0.3 broadcast_in_dim.18
  9.3 1.1 bitcast_dynamic-update-slice_fusion.2
  10.4 7.6 %collective-permute-done.22 = bf16[160,2048]{1,0:T(8,128)(2,1)} collective-permute-done((bf16[160,2048]{1,0:T(8,128)(2,1)}, bf16[160,2048]{1,0:T(8,128)(2,1)}, u32[]{:S(2)}, u32[]{:S(2)}) %collective-permute-start.22) | collective-permute-done | bytes 655392 | tf_op jit(solution)/shard_map/ppermute | solution.py:180
  18.0 1.0 slice.88
  19.0 3.7 %collective-permute-start.23 = (bf16[80,2048]{1,0:T(8,128)(2,1)S(1)}, bf16[80,2048]{1,0:T(8,128)(2,1)S(1)}, u32[]{:S(2)}, u32[]{:S(2)}) collective-permute-start(bf16[80,2048]{1,0:T(8,128)(2,1)S(1)} %slice.88), channel_id=1, source_target_pairs={{0,1},{1,2},{2,3},{3,0},{4,5},{5,6},{6,7},{7,4},{8,9},{9,10},{10,1... | collective-permute-start | bytes 983048 | tf_op jit(solution)/shard_map/ppermute | solution.py:180
  22.8 0.1 collective-permute-start.24
  22.9 0.1 bitcast_dynamic-update-slice_fusion.1
  22.9 1.1 bitcast_dynamic-update-slice_fusion
  24.1 4.5 %collective-permute-done.23 = bf16[80,2048]{1,0:T(8,128)(2,1)S(1)} collective-permute-done((bf16[80,2048]{1,0:T(8,128)(2,1)S(1)}, bf16[80,2048]{1,0:T(8,128)(2,1)S(1)}, u32[]{:S(2)}, u32[]{:S(2)}) %collective-permute-start.23) | collective-permute-done | bytes 327712 | tf_op jit(solution)/shard_map/ppermute | solution.py:180
  28.6 3.5 %collective-permute-done.24 = bf16[80,2048]{1,0:T(8,128)(2,1)S(1)} collective-permute-done((bf16[80,2048]{1,0:T(8,128)(2,1)S(1)}, bf16[80,2048]{1,0:T(8,128)(2,1)S(1)}, u32[]{:S(2)}, u32[]{:S(2)}) %collective-permute-start.24) | collective-permute-done | bytes 327712 | tf_op jit(solution)/shard_map/ppermute | solution.py:180
  32.1 1.5 copy-done
  33.7 9.5 %grad_term.1 = (bf16[4,8,32,1408]{3,2,1,0:T(8,128)(2,1)}, bf16[4,8,32,1408]{3,2,1,0:T(8,128)(2,1)}) custom-call(s32[4]{0:T(128)} %pad_add_fusion.where, bf16[640,2048]{1,0:T(8,128)(2,1)} %bitcast.78, bf16[640,1408]{1,0:T(8,128)(2,1)} %fusion.16.hidden), custom_call_target="tpu_custom_call" | custom-call | flops 3690987520 | bytes 12582912 | tf_op jit(solution)/shard_map/grad_term/pallas_call | solution.py:44
  43.2 1.7 collective-permute-start.2
  44.8 2.9 %collective-permute-start.1 = (bf16[32,1408]{1,0:T(8,128)(2,1)S(1)}, bf16[32,1408]{1,0:T(8,128)(2,1)S(1)}, u32[]{:S(2)}, u32[]{:S(2)}) collective-permute-start(bf16[32,1408]{1,0:T(8,128)(2,1)S(1)} %bitcast.82), channel_id=1, source_target_pairs={{0,16},{4,20},{8,24},{12,28},{16,0},{20,4},{24,8},{28,12},{32,48},... | collective-permute-start | bytes 270344 | tf_op jit(solution)/shard_map/ppermute | solution.py:176
  47.7 1.3 collective-permute-start
  49.1 0.4 collective-permute-done.2
  49.5 3.1 %collective-permute-done.1 = bf16[32,1408]{1,0:T(8,128)(2,1)S(1)} collective-permute-done((bf16[32,1408]{1,0:T(8,128)(2,1)S(1)}, bf16[32,1408]{1,0:T(8,128)(2,1)S(1)}, u32[]{:S(2)}, u32[]{:S(2)}) %collective-permute-start.1) | collective-permute-done | bytes 90144 | tf_op jit(solution)/shard_map/ppermute | solution.py:176
  52.6 0.1 pad_maximum_fusion.refs_0_
  52.7 2.0 %collective-permute-start.6 = (bf16[4,32,1408]{2,1,0:T(8,128)(2,1)S(1)}, bf16[4,32,1408]{2,1,0:T(8,128)(2,1)S(1)}, u32[]{:S(2)}, u32[]{:S(2)}) collective-permute-start(bf16[4,32,1408]{2,1,0:T(8,128)(2,1)S(1)} %pad_maximum_fusion.refs_0_), channel_id=1, source_target_pairs={{0,32},{4,36},{8,40},{12,44},{16,48},{20,52},{24,56},{28,60},{32,6... | collective-permute-start | bytes 1081352 | tf_op jit(solution)/shard_map/ppermute | solution.py:176
  54.7 4.0 %collective-permute-start.3 = (bf16[4,32,1408]{2,1,0:T(8,128)(2,1)S(1)}, bf16[4,32,1408]{2,1,0:T(8,128)(2,1)S(1)}, u32[]{:S(2)}, u32[]{:S(2)}) collective-permute-start(bf16[4,32,1408]{2,1,0:T(8,128)(2,1)S(1)} %pad_maximum_fusion.refs_0_), channel_id=1, source_target_pairs={{0,224},{4,228},{8,232},{12,236},{16,240},{20,244},{24,248},{28,25... | collective-permute-start | bytes 1081352 | tf_op jit(solution)/shard_map/ppermute | solution.py:176
  58.7 8.1 %collective-permute-done.6.refs_7_ = bf16[4,32,1408]{2,1,0:T(8,128)(2,1)S(1)} collective-permute-done((bf16[4,32,1408]{2,1,0:T(8,128)(2,1)S(1)}, bf16[4,32,1408]{2,1,0:T(8,128)(2,1)S(1)}, u32[]{:S(2)}, u32[]{:S(2)}) %collective-permute-start.6) | collective-permute-done | bytes 360480 | tf_op jit(solution)/shard_map/ppermute | solution.py:176
  66.8 0.0 copy-start.3
  66.8 2.6 %fusion.19 = (bf16[8,32,1408]{2,1,0:T(8,128)(2,1)S(1)}, f32[1,8,32,1408]{3,2,1,0:T(8,128)S(1)}, bf16[8,32,1408]{2,1,0:T(8,128)(2,1)S(1)}, f32[1,8,32,1408]{3,2,1,0:T(8,128)S(1)}) fusion(bf16[4,8,32,1408]{3,2,1,0:T(8,128)(2,1)S(1)} %collective-permute-done.25, bf16[4,8,32,1408]{3,2,1,0:T(8,128)(2,1)} %get-tuple-element.20), kind=kLoop, calls=%fused_computation.47 | loop fusion | flops 5046272 | bytes 10092544 | tf_op jit(solution)/shard_map/convert_element_type | solution.py:235
  69.4 0.0 copy-start.2
  69.4 0.3 collective-permute-start.27
  69.7 3.0 %collective-permute-start.26 = (bf16[8,32,1408]{2,1,0:T(8,128)(2,1)S(1)}, bf16[8,32,1408]{2,1,0:T(8,128)(2,1)S(1)}, u32[]{:S(2)}, u32[]{:S(2)}) collective-permute-start(bf16[8,32,1408]{2,1,0:T(8,128)(2,1)S(1)} %get-tuple-element.24), channel_id=1, source_target_pairs={{0,24},{4,28},{8,0},{12,4},{16,8},{20,12},{24,16},{28,20},{32,56},... | collective-permute-start | bytes 2162696 | tf_op jit(solution)/shard_map/ppermute | solution.py:176
  72.7 3.2 %collective-permute-start.4 = (bf16[4,32,1408]{2,1,0:T(8,128)(2,1)S(1)}, bf16[4,32,1408]{2,1,0:T(8,128)(2,1)S(1)}, u32[]{:S(2)}, u32[]{:S(2)}) collective-permute-start(bf16[4,32,1408]{2,1,0:T(8,128)(2,1)S(1)} %collective-permute-done.3.refs_1_), channel_id=1, source_target_pairs={{0,224},{4,228},{8,232},{12,236},{16,240},{20,244},{24,248},{28,25... | collective-permute-start | bytes 1081352 | tf_op jit(solution)/shard_map/ppermute | solution.py:176
  75.9 1.4 collective-permute-done.7.refs_6_
  77.3 4.6 %collective-permute-done.4.refs_2_ = bf16[4,32,1408]{2,1,0:T(8,128)(2,1)S(1)} collective-permute-done((bf16[4,32,1408]{2,1,0:T(8,128)(2,1)S(1)}, bf16[4,32,1408]{2,1,0:T(8,128)(2,1)S(1)}, u32[]{:S(2)}, u32[]{:S(2)}) %collective-permute-start.4) | collective-permute-done | bytes 360480 | tf_op jit(solution)/shard_map/ppermute | solution.py:176
  81.9 3.8 %collective-permute-start.5 = (bf16[4,32,1408]{2,1,0:T(8,128)(2,1)S(1)}, bf16[4,32,1408]{2,1,0:T(8,128)(2,1)S(1)}, u32[]{:S(2)}, u32[]{:S(2)}) collective-permute-start(bf16[4,32,1408]{2,1,0:T(8,128)(2,1)S(1)} %collective-permute-done.4.refs_2_), channel_id=1, source_target_pairs={{0,224},{4,228},{8,232},{12,236},{16,240},{20,244},{24,248},{28,25... | collective-permute-start | bytes 1081352 | tf_op jit(solution)/shard_map/ppermute | solution.py:176
  85.7 2.3 %collective-permute-done.8.refs_5_ = bf16[4,32,1408]{2,1,0:T(8,128)(2,1)S(1)} collective-permute-done((bf16[4,32,1408]{2,1,0:T(8,128)(2,1)S(1)}, bf16[4,32,1408]{2,1,0:T(8,128)(2,1)S(1)}, u32[]{:S(2)}, u32[]{:S(2)}) %collective-permute-start.8) | collective-permute-done | bytes 360480 | tf_op jit(solution)/shard_map/ppermute | solution.py:176
  88.0 0.5 collective-permute-start.16
  88.5 1.1 fusion.26
  89.6 0.3 collective-permute-start.15
  89.9 4.0 %collective-permute-done.5.refs_3_ = bf16[4,32,1408]{2,1,0:T(8,128)(2,1)S(1)} collective-permute-done((bf16[4,32,1408]{2,1,0:T(8,128)(2,1)S(1)}, bf16[4,32,1408]{2,1,0:T(8,128)(2,1)S(1)}, u32[]{:S(2)}, u32[]{:S(2)}) %collective-permute-start.5) | collective-permute-done | bytes 360480 | tf_op jit(solution)/shard_map/ppermute | solution.py:176
  94.0 6.1 %collective-permute-done.9.refs_4_ = bf16[4,32,1408]{2,1,0:T(8,128)(2,1)S(1)} collective-permute-done((bf16[4,32,1408]{2,1,0:T(8,128)(2,1)S(1)}, bf16[4,32,1408]{2,1,0:T(8,128)(2,1)S(1)}, u32[]{:S(2)}, u32[]{:S(2)}) %collective-permute-start.9) | collective-permute-done | bytes 360480 | tf_op jit(solution)/shard_map/ppermute | solution.py:176
  100.1 0.1 collective-permute-start.28
  100.3 3.5 %collective-permute-start.29 = (bf16[4,32,1408]{2,1,0:T(8,128)(2,1)}, bf16[4,32,1408]{2,1,0:T(8,128)(2,1)}, u32[]{:S(2)}, u32[]{:S(2)}) collective-permute-start(bf16[4,32,1408]{2,1,0:T(8,128)(2,1)} %get-tuple-element.31), channel_id=1, source_target_pairs={{0,24},{4,28},{8,0},{12,4},{16,8},{20,12},{24,16},{28,20},{32,56},... | collective-permute-start | bytes 1081352 | tf_op jit(solution)/shard_map/ppermute | solution.py:176
  103.8 2.4 %fusion.17 = bf16[640,1408]{1,0:T(8,128)(2,1)} fusion(bf16[640,1408]{1,0:T(8,128)(2,1)S(1)} %copy-done.2, bf16[640,1408]{1,0:T(8,128)(2,1)S(1)} %copy-done.3), kind=kLoop, calls=%fused_computation.24 | loop fusion | flops 7208960 | bytes 5406720 | tf_op jit(solution)/shard_map/convert_element_type | solution.py:211
  106.2 0.7 copy-done.25
  106.9 0.1 copy-done.24
  107.0 11.6 %partial_products.1 = (bf16[160,2048]{1,0:T(8,128)(2,1)}, bf16[160,2048]{1,0:T(8,128)(2,1)}, bf16[160,2048]{1,0:T(8,128)(2,1)}, bf16[160,2048]{1,0:T(8,128)(2,1)}, bf16[8,4,2,32,1408]{4,3,2,1,0:T(8,128)(2,1)}) custom-call(s32[4]{0:T(128)} %pad_add_fusion.where, bf16[4,160,1408]{2,1,0:T(8,128)(2,1)} %bitcast.80, bf16[4,32,1408]{2,1,0:T(8,128)(2,1)} %copy-done.9, ...), custom_call_target="tpu_custom_call" | custom-call | flops 3690987520 | bytes 16777216 | tf_op jit(solution)/shard_map/partial_products/pallas_call | solution.py:133
  118.6 0.1 collective-permute-start.20
  118.7 3.2 %collective-permute-start.19 = (bf16[160,2048]{1,0:T(8,128)(2,1)}, bf16[160,2048]{1,0:T(8,128)(2,1)S(1)}, u32[]{:S(2)}, u32[]{:S(2)}) collective-permute-start(bf16[160,2048]{1,0:T(8,128)(2,1)} %get-tuple-element.15), channel_id=1, source_target_pairs={{0,1},{1,2},{2,3},{3,0},{4,5},{5,6},{6,7},{7,4},{8,9},{9,10},{10,1... | collective-permute-start | bytes 1966088 | tf_op jit(solution)/shard_map/ppermute | solution.py:180
  121.9 1.7 fusion.29
  123.6 0.1 fusion.52
  123.7 1.5 collective-permute-start.36
  125.2 0.3 fusion.51
  125.4 0.7 collective-permute-start.35
  126.1 9.2 %fusion.15 = (bf16[640,1408]{1,0:T(8,128)(2,1)}, bf16[640,1408]{1,0:T(8,128)(2,1)}) fusion(bf16[640,1408]{1,0:T(8,128)(2,1)S(1)} %copy-done.4, bf16[640,1408]{1,0:T(8,128)(2,1)S(1)} %copy-done.5, bf16[640,2048]{1,0:T(8,128)(2,1)S(1)} %bitcast.79, bf16[2048,1408]{1,0:T(8,128)(2,1)} %bitcast.88), kind=kOutput, calls=%fused_computation.22 | convolution fusion | flops 3704504320 | bytes 15597568 | tf_op jit(solution)/shard_map/dot_general | solution.py:263
  135.4 15.2 %collective-permute-done.20 = bf16[160,2048]{1,0:T(8,128)(2,1)S(1)} collective-permute-done((bf16[160,2048]{1,0:T(8,128)(2,1)}, bf16[160,2048]{1,0:T(8,128)(2,1)S(1)}, u32[]{:S(2)}, u32[]{:S(2)}) %collective-permute-start.20) | collective-permute-done | bytes 655392 | tf_op jit(solution)/shard_map/ppermute | solution.py:180
  150.6 1.0 collective-permute-start.34
  151.7 1.9 %collective-permute-start.33 = (bf16[32,1408]{1,0:T(8,128)(2,1)S(1)}, bf16[32,1408]{1,0:T(8,128)(2,1)S(1)}, u32[]{:S(2)}, u32[]{:S(2)}) collective-permute-start(bf16[32,1408]{1,0:T(8,128)(2,1)S(1)} %get-tuple-element.35), channel_id=1, source_target_pairs={{0,64},{4,68},{8,72},{12,76},{16,80},{20,84},{24,88},{28,92},{32,9... | collective-permute-start | bytes 270344 | tf_op jit(solution)/shard_map/ppermute | solution.py:176
  153.5 2.5 %collective-permute-start.32 = (bf16[32,1408]{1,0:T(8,128)(2,1)S(1)}, bf16[32,1408]{1,0:T(8,128)(2,1)S(1)}, u32[]{:S(2)}, u32[]{:S(2)}) collective-permute-start(bf16[32,1408]{1,0:T(8,128)(2,1)S(1)} %get-tuple-element.34), channel_id=1, source_target_pairs={{0,160},{4,164},{8,168},{12,172},{16,176},{20,180},{24,184},{28,18... | collective-permute-start | bytes 270344 | tf_op jit(solution)/shard_map/ppermute | solution.py:176
  156.1 1.5 collective-permute-start.31
  157.5 4.1 %collective-permute-start.30 = (bf16[32,1408]{1,0:T(8,128)(2,1)S(1)}, bf16[32,1408]{1,0:T(8,128)(2,1)S(1)}, u32[]{:S(2)}, u32[]{:S(2)}) collective-permute-start(bf16[32,1408]{1,0:T(8,128)(2,1)S(1)} %get-tuple-element.32), channel_id=1, source_target_pairs={{0,128},{4,132},{8,136},{12,140},{16,144},{20,148},{24,152},{28,15... | collective-permute-start | bytes 270344 | tf_op jit(solution)/shard_map/ppermute | solution.py:176
  161.7 1.3 add_convert_fusion.2
  163.0 4.2 %collective-permute-done.31 = bf16[32,1408]{1,0:T(8,128)(2,1)S(1)} collective-permute-done((bf16[32,1408]{1,0:T(8,128)(2,1)S(1)}, bf16[32,1408]{1,0:T(8,128)(2,1)S(1)}, u32[]{:S(2)}, u32[]{:S(2)}) %collective-permute-start.31) | collective-permute-done | bytes 90144 | tf_op jit(solution)/shard_map/ppermute | solution.py:176
  167.2 3.3 %collective-permute-done.30 = bf16[32,1408]{1,0:T(8,128)(2,1)S(1)} collective-permute-done((bf16[32,1408]{1,0:T(8,128)(2,1)S(1)}, bf16[32,1408]{1,0:T(8,128)(2,1)S(1)}, u32[]{:S(2)}, u32[]{:S(2)}) %collective-permute-start.30) | collective-permute-done | bytes 90144 | tf_op jit(solution)/shard_map/ppermute | solution.py:176
  170.5 0.8 fusion.37
  (84 shorter events, 0.3 us)
Async XLA Ops:
  0.6 22.1 %collective-permute-start.21 = (bf16[160,2048]{1,0:T(8,128)(2,1)}, bf16[160,2048]{1,0:T(8,128)(2,1)S(1)}, u32[]{:S(2)}, u32[]{:S(2)}) collective-permute-start(bf16[160,2048]{1,0:T(8,128)(2,1)} %param.11), channel_id=1, source_target_pairs={{0,3},{1,0},{2,1},{3,2},{4,7},{5,4},{6,5},{7,6},{8,11},{9,8},{10,9... | collective-permute-start | bytes 1966088 | tf_op jit(solution)/shard_map/ppermute | solution.py:180
  1.5 16.5 %collective-permute-start.22 = (bf16[160,2048]{1,0:T(8,128)(2,1)}, bf16[160,2048]{1,0:T(8,128)(2,1)}, u32[]{:S(2)}, u32[]{:S(2)}) collective-permute-start(bf16[160,2048]{1,0:T(8,128)(2,1)} %param.11), channel_id=1, source_target_pairs={{0,1},{1,2},{2,3},{3,0},{4,5},{5,6},{6,7},{7,4},{8,9},{9,10},{10,1... | collective-permute-start | bytes 1966088 | tf_op jit(solution)/shard_map/ppermute | solution.py:180
  19.0 9.5 %collective-permute-start.23 = (bf16[80,2048]{1,0:T(8,128)(2,1)S(1)}, bf16[80,2048]{1,0:T(8,128)(2,1)S(1)}, u32[]{:S(2)}, u32[]{:S(2)}) collective-permute-start(bf16[80,2048]{1,0:T(8,128)(2,1)S(1)} %slice.88), channel_id=1, source_target_pairs={{0,1},{1,2},{2,3},{3,0},{4,5},{5,6},{6,7},{7,4},{8,9},{9,10},{10,1... | collective-permute-start | bytes 983048 | tf_op jit(solution)/shard_map/ppermute | solution.py:180
  22.8 9.3 %collective-permute-start.24 = (bf16[80,2048]{1,0:T(8,128)(2,1)S(1)}, bf16[80,2048]{1,0:T(8,128)(2,1)S(1)}, u32[]{:S(2)}, u32[]{:S(2)}) collective-permute-start(bf16[80,2048]{1,0:T(8,128)(2,1)S(1)} %slice.89), channel_id=1, source_target_pairs={{0,3},{1,0},{2,1},{3,2},{4,7},{5,4},{6,5},{7,6},{8,11},{9,8},{10,9... | collective-permute-start | bytes 983048 | tf_op jit(solution)/shard_map/ppermute | solution.py:180
  32.1 1.5 copy-start
  33.7 9.5 %copy-start.11 = (bf16[1408,32]{0,1:T(8,128)(2,1)S(1)}, bf16[1408,32]{0,1:T(8,128)(2,1)}, u32[]{:S(2)}) copy-start(bf16[1408,32]{0,1:T(8,128)(2,1)} %param.12) | copy-start | bytes 270340
  43.2 23.6 %collective-permute-start.25 = (bf16[4,8,32,1408]{3,2,1,0:T(8,128)(2,1)}, bf16[4,8,32,1408]{3,2,1,0:T(8,128)(2,1)S(1)}, u32[]{:S(2)}, u32[]{:S(2)}) collective-permute-start(bf16[4,8,32,1408]{3,2,1,0:T(8,128)(2,1)} %get-tuple-element.21), channel_id=1, source_target_pairs={{0,4},{4,0},{8,12},{12,8},{16,20},{20,16},{24,28},{28,24},{32,36},... | collective-permute-start | bytes 8650760 | tf_op jit(solution)/shard_map/ppermute | solution.py:176
  43.2 6.3 %collective-permute-start.2 = (bf16[32,1408]{1,0:T(8,128)(2,1)S(1)}, bf16[32,1408]{1,0:T(8,128)(2,1)S(1)}, u32[]{:S(2)}, u32[]{:S(2)}) collective-permute-start(bf16[32,1408]{1,0:T(8,128)(2,1)S(1)} %bitcast.81), channel_id=1, source_target_pairs={{0,8},{4,12},{8,16},{12,20},{16,24},{20,28},{24,0},{28,4},{32,40},... | collective-permute-start | bytes 270344 | tf_op jit(solution)/shard_map/ppermute | solution.py:176
  44.8 7.8 %collective-permute-start.1 = (bf16[32,1408]{1,0:T(8,128)(2,1)S(1)}, bf16[32,1408]{1,0:T(8,128)(2,1)S(1)}, u32[]{:S(2)}, u32[]{:S(2)}) collective-permute-start(bf16[32,1408]{1,0:T(8,128)(2,1)S(1)} %bitcast.82), channel_id=1, source_target_pairs={{0,16},{4,20},{8,24},{12,28},{16,0},{20,4},{24,8},{28,12},{32,48},... | collective-permute-start | bytes 270344 | tf_op jit(solution)/shard_map/ppermute | solution.py:176
  47.7 4.9 %collective-permute-start = (bf16[32,1408]{1,0:T(8,128)(2,1)S(1)}, bf16[32,1408]{1,0:T(8,128)(2,1)S(1)}, u32[]{:S(2)}, u32[]{:S(2)}) collective-permute-start(bf16[32,1408]{1,0:T(8,128)(2,1)S(1)} %bitcast.83), channel_id=1, source_target_pairs={{0,24},{4,28},{8,0},{12,4},{16,8},{20,12},{24,16},{28,20},{32,56},... | collective-permute-start | bytes 270344 | tf_op jit(solution)/shard_map/ppermute | solution.py:176
  52.7 16.7 %copy-start.9 = (bf16[4,32,1408]{2,1,0:T(8,128)(2,1)}, bf16[4,32,1408]{2,1,0:T(8,128)(2,1)S(1)}, u32[]{:S(2)}) copy-start(bf16[4,32,1408]{2,1,0:T(8,128)(2,1)S(1)} %pad_maximum_fusion.refs_0_) | copy-start | bytes 1081348
  52.7 14.1 %collective-permute-start.6 = (bf16[4,32,1408]{2,1,0:T(8,128)(2,1)S(1)}, bf16[4,32,1408]{2,1,0:T(8,128)(2,1)S(1)}, u32[]{:S(2)}, u32[]{:S(2)}) collective-permute-start(bf16[4,32,1408]{2,1,0:T(8,128)(2,1)S(1)} %pad_maximum_fusion.refs_0_), channel_id=1, source_target_pairs={{0,32},{4,36},{8,40},{12,44},{16,48},{20,52},{24,56},{28,60},{32,6... | collective-permute-start | bytes 1081352 | tf_op jit(solution)/shard_map/ppermute | solution.py:176
  54.7 18.0 %collective-permute-start.3 = (bf16[4,32,1408]{2,1,0:T(8,128)(2,1)S(1)}, bf16[4,32,1408]{2,1,0:T(8,128)(2,1)S(1)}, u32[]{:S(2)}, u32[]{:S(2)}) collective-permute-start(bf16[4,32,1408]{2,1,0:T(8,128)(2,1)S(1)} %pad_maximum_fusion.refs_0_), channel_id=1, source_target_pairs={{0,224},{4,228},{8,232},{12,236},{16,240},{20,244},{24,248},{28,25... | collective-permute-start | bytes 1081352 | tf_op jit(solution)/shard_map/ppermute | solution.py:176
  58.7 17.2 %collective-permute-start.10 = (bf16[4,32,1408]{2,1,0:T(8,128)(2,1)S(1)}, bf16[4,32,1408]{2,1,0:T(8,128)(2,1)S(1)}, u32[]{:S(2)}, u32[]{:S(2)}) collective-permute-start(bf16[4,32,1408]{2,1,0:T(8,128)(2,1)S(1)} %pad_maximum_fusion.refs_0_), channel_id=1, source_target_pairs={{0,4},{4,0},{8,12},{12,8},{16,20},{20,16},{24,28},{28,24},{32,36},... | collective-permute-start | bytes 1081352 | tf_op jit(solution)/shard_map/ppermute | solution.py:176
  66.8 15.1 %copy-start.12 = (bf16[4,32,1408]{2,1,0:T(8,128)(2,1)}, bf16[4,32,1408]{2,1,0:T(8,128)(2,1)S(1)}, u32[]{:S(2)}) copy-start(bf16[4,32,1408]{2,1,0:T(8,128)(2,1)S(1)} %collective-permute-done.6.refs_7_) | copy-start | bytes 1081348
  66.8 10.5 %collective-permute-start.7 = (bf16[4,32,1408]{2,1,0:T(8,128)(2,1)S(1)}, bf16[4,32,1408]{2,1,0:T(8,128)(2,1)S(1)}, u32[]{:S(2)}, u32[]{:S(2)}) collective-permute-start(bf16[4,32,1408]{2,1,0:T(8,128)(2,1)S(1)} %collective-permute-done.6.refs_7_), channel_id=1, source_target_pairs={{0,32},{4,36},{8,40},{12,44},{16,48},{20,52},{24,56},{28,60},{32,6... | collective-permute-start | bytes 1081352 | tf_op jit(solution)/shard_map/ppermute | solution.py:176
  66.8 37.0 %copy-start.3 = (bf16[640,1408]{1,0:T(8,128)(2,1)S(1)}, bf16[640,1408]{1,0:T(8,128)(2,1)}, u32[]{:S(2)}) copy-start(bf16[640,1408]{1,0:T(8,128)(2,1)} %param.7) | copy-start | bytes 5406724
  69.4 34.4 %copy-start.2 = (bf16[640,1408]{1,0:T(8,128)(2,1)S(1)}, bf16[640,1408]{1,0:T(8,128)(2,1)}, u32[]{:S(2)}) copy-start(bf16[640,1408]{1,0:T(8,128)(2,1)} %param.8) | copy-start | bytes 5406724
  69.4 18.6 %collective-permute-start.27 = (bf16[8,32,1408]{2,1,0:T(8,128)(2,1)S(1)}, bf16[8,32,1408]{2,1,0:T(8,128)(2,1)S(1)}, u32[]{:S(2)}, u32[]{:S(2)}) collective-permute-start(bf16[8,32,1408]{2,1,0:T(8,128)(2,1)S(1)} %get-tuple-element.22), channel_id=1, source_target_pairs={{0,8},{4,12},{8,16},{12,20},{16,24},{20,28},{24,0},{28,4},{32,40},... | collective-permute-start | bytes 2162696 | tf_op jit(solution)/shard_map/ppermute | solution.py:176
  69.7 18.8 %collective-permute-start.26 = (bf16[8,32,1408]{2,1,0:T(8,128)(2,1)S(1)}, bf16[8,32,1408]{2,1,0:T(8,128)(2,1)S(1)}, u32[]{:S(2)}, u32[]{:S(2)}) collective-permute-start(bf16[8,32,1408]{2,1,0:T(8,128)(2,1)S(1)} %get-tuple-element.24), channel_id=1, source_target_pairs={{0,24},{4,28},{8,0},{12,4},{16,8},{20,12},{24,16},{28,20},{32,56},... | collective-permute-start | bytes 2162696 | tf_op jit(solution)/shard_map/ppermute | solution.py:176
  72.7 17.2 %copy-start.13 = (bf16[4,32,1408]{2,1,0:T(8,128)(2,1)}, bf16[4,32,1408]{2,1,0:T(8,128)(2,1)S(1)}, u32[]{:S(2)}) copy-start(bf16[4,32,1408]{2,1,0:T(8,128)(2,1)S(1)} %collective-permute-done.3.refs_1_) | copy-start | bytes 1081348
  72.7 9.2 %collective-permute-start.4 = (bf16[4,32,1408]{2,1,0:T(8,128)(2,1)S(1)}, bf16[4,32,1408]{2,1,0:T(8,128)(2,1)S(1)}, u32[]{:S(2)}, u32[]{:S(2)}) collective-permute-start(bf16[4,32,1408]{2,1,0:T(8,128)(2,1)S(1)} %collective-permute-done.3.refs_1_), channel_id=1, source_target_pairs={{0,224},{4,228},{8,232},{12,236},{16,240},{20,244},{24,248},{28,25... | collective-permute-start | bytes 1081352 | tf_op jit(solution)/shard_map/ppermute | solution.py:176
  75.9 18.0 %copy-start.14 = (bf16[4,32,1408]{2,1,0:T(8,128)(2,1)}, bf16[4,32,1408]{2,1,0:T(8,128)(2,1)S(1)}, u32[]{:S(2)}) copy-start(bf16[4,32,1408]{2,1,0:T(8,128)(2,1)S(1)} %collective-permute-done.10.refs_8_) | copy-start | bytes 1081348
  75.9 6.0 %collective-permute-start.11 = (bf16[4,32,1408]{2,1,0:T(8,128)(2,1)S(1)}, bf16[4,32,1408]{2,1,0:T(8,128)(2,1)S(1)}, u32[]{:S(2)}, u32[]{:S(2)}) collective-permute-start(bf16[4,32,1408]{2,1,0:T(8,128)(2,1)S(1)} %collective-permute-done.3.refs_1_), channel_id=1, source_target_pairs={{0,4},{4,0},{8,12},{12,8},{16,20},{20,16},{24,28},{28,24},{32,36},... | collective-permute-start | bytes 1081352 | tf_op jit(solution)/shard_map/ppermute | solution.py:176
  77.3 16.7 %copy-start.15 = (bf16[4,32,1408]{2,1,0:T(8,128)(2,1)}, bf16[4,32,1408]{2,1,0:T(8,128)(2,1)S(1)}, u32[]{:S(2)}) copy-start(bf16[4,32,1408]{2,1,0:T(8,128)(2,1)S(1)} %collective-permute-done.7.refs_6_) | copy-start | bytes 1081348
  77.3 10.7 %collective-permute-start.8 = (bf16[4,32,1408]{2,1,0:T(8,128)(2,1)S(1)}, bf16[4,32,1408]{2,1,0:T(8,128)(2,1)S(1)}, u32[]{:S(2)}, u32[]{:S(2)}) collective-permute-start(bf16[4,32,1408]{2,1,0:T(8,128)(2,1)S(1)} %collective-permute-done.7.refs_6_), channel_id=1, source_target_pairs={{0,32},{4,36},{8,40},{12,44},{16,48},{20,52},{24,56},{28,60},{32,6... | collective-permute-start | bytes 1081352 | tf_op jit(solution)/shard_map/ppermute | solution.py:176
  81.9 18.3 %copy-start.16 = (bf16[4,32,1408]{2,1,0:T(8,128)(2,1)}, bf16[4,32,1408]{2,1,0:T(8,128)(2,1)S(1)}, u32[]{:S(2)}) copy-start(bf16[4,32,1408]{2,1,0:T(8,128)(2,1)S(1)} %collective-permute-done.4.refs_2_) | copy-start | bytes 1081348
  81.9 7.7 %collective-permute-start.17 = (bf16[4,32,1408]{2,1,0:T(8,128)(2,1)S(1)}, bf16[4,32,1408]{2,1,0:T(8,128)(2,1)S(1)}, u32[]{:S(2)}, u32[]{:S(2)}) collective-permute-start(bf16[4,32,1408]{2,1,0:T(8,128)(2,1)S(1)} %collective-permute-done.6.refs_7_), channel_id=1, source_target_pairs={{0,4},{4,0},{8,12},{12,8},{16,20},{20,16},{24,28},{28,24},{32,36},... | collective-permute-start | bytes 1081352 | tf_op jit(solution)/shard_map/ppermute | solution.py:176
  81.9 18.3 %copy-start.17 = (bf16[4,32,1408]{2,1,0:T(8,128)(2,1)}, bf16[4,32,1408]{2,1,0:T(8,128)(2,1)S(1)}, u32[]{:S(2)}) copy-start(bf16[4,32,1408]{2,1,0:T(8,128)(2,1)S(1)} %collective-permute-done.11.refs_9_) | copy-start | bytes 1081348
  81.9 12.0 %collective-permute-start.5 = (bf16[4,32,1408]{2,1,0:T(8,128)(2,1)S(1)}, bf16[4,32,1408]{2,1,0:T(8,128)(2,1)S(1)}, u32[]{:S(2)}, u32[]{:S(2)}) collective-permute-start(bf16[4,32,1408]{2,1,0:T(8,128)(2,1)S(1)} %collective-permute-done.4.refs_2_), channel_id=1, source_target_pairs={{0,224},{4,228},{8,232},{12,236},{16,240},{20,244},{24,248},{28,25... | collective-permute-start | bytes 1081352 | tf_op jit(solution)/shard_map/ppermute | solution.py:176
  87.9 18.2 %copy-start.18 = (bf16[4,32,1408]{2,1,0:T(8,128)(2,1)}, bf16[4,32,1408]{2,1,0:T(8,128)(2,1)S(1)}, u32[]{:S(2)}) copy-start(bf16[4,32,1408]{2,1,0:T(8,128)(2,1)S(1)} %collective-permute-done.8.refs_5_) | copy-start | bytes 1081348
  87.9 12.2 %collective-permute-start.12 = (bf16[4,32,1408]{2,1,0:T(8,128)(2,1)S(1)}, bf16[4,32,1408]{2,1,0:T(8,128)(2,1)S(1)}, u32[]{:S(2)}, u32[]{:S(2)}) collective-permute-start(bf16[4,32,1408]{2,1,0:T(8,128)(2,1)S(1)} %collective-permute-done.4.refs_2_), channel_id=1, source_target_pairs={{0,4},{4,0},{8,12},{12,8},{16,20},{20,16},{24,28},{28,24},{32,36},... | collective-permute-start | bytes 1081352 | tf_op jit(solution)/shard_map/ppermute | solution.py:176
  88.0 1.6 copy-start.6
  88.0 12.2 %collective-permute-start.16 = (bf16[4,32,1408]{2,1,0:T(8,128)(2,1)S(1)}, bf16[4,32,1408]{2,1,0:T(8,128)(2,1)S(1)}, u32[]{:S(2)}, u32[]{:S(2)}) collective-permute-start(bf16[4,32,1408]{2,1,0:T(8,128)(2,1)S(1)} %collective-permute-done.7.refs_6_), channel_id=1, source_target_pairs={{0,4},{4,0},{8,12},{12,8},{16,20},{20,16},{24,28},{28,24},{32,36},... | collective-permute-start | bytes 1081352 | tf_op jit(solution)/shard_map/ppermute | solution.py:176
  88.5 1.1 copy-start.7
  88.5 11.6 %collective-permute-start.9 = (bf16[4,32,1408]{2,1,0:T(8,128)(2,1)S(1)}, bf16[4,32,1408]{2,1,0:T(8,128)(2,1)S(1)}, u32[]{:S(2)}, u32[]{:S(2)}) collective-permute-start(bf16[4,32,1408]{2,1,0:T(8,128)(2,1)S(1)} %collective-permute-done.8.refs_5_), channel_id=1, source_target_pairs={{0,32},{4,36},{8,40},{12,44},{16,48},{20,52},{24,56},{28,60},{32,6... | collective-permute-start | bytes 1081352 | tf_op jit(solution)/shard_map/ppermute | solution.py:176
  89.6 14.2 %copy-start.19 = (bf16[4,32,1408]{2,1,0:T(8,128)(2,1)}, bf16[4,32,1408]{2,1,0:T(8,128)(2,1)S(1)}, u32[]{:S(2)}) copy-start(bf16[4,32,1408]{2,1,0:T(8,128)(2,1)S(1)} %collective-permute-done.17.refs_15_) | copy-start | bytes 1081348
  89.6 16.5 %collective-permute-start.15 = (bf16[4,32,1408]{2,1,0:T(8,128)(2,1)S(1)}, bf16[4,32,1408]{2,1,0:T(8,128)(2,1)S(1)}, u32[]{:S(2)}, u32[]{:S(2)}) collective-permute-start(bf16[4,32,1408]{2,1,0:T(8,128)(2,1)S(1)} %collective-permute-done.8.refs_5_), channel_id=1, source_target_pairs={{0,4},{4,0},{8,12},{12,8},{16,20},{20,16},{24,28},{28,24},{32,36},... | collective-permute-start | bytes 1081352 | tf_op jit(solution)/shard_map/ppermute | solution.py:176
  93.9 12.2 %copy-start.20 = (bf16[4,32,1408]{2,1,0:T(8,128)(2,1)}, bf16[4,32,1408]{2,1,0:T(8,128)(2,1)S(1)}, u32[]{:S(2)}) copy-start(bf16[4,32,1408]{2,1,0:T(8,128)(2,1)S(1)} %collective-permute-done.5.refs_3_) | copy-start | bytes 1081348
  93.9 12.2 %collective-permute-start.13 = (bf16[4,32,1408]{2,1,0:T(8,128)(2,1)S(1)}, bf16[4,32,1408]{2,1,0:T(8,128)(2,1)S(1)}, u32[]{:S(2)}, u32[]{:S(2)}) collective-permute-start(bf16[4,32,1408]{2,1,0:T(8,128)(2,1)S(1)} %collective-permute-done.5.refs_3_), channel_id=1, source_target_pairs={{0,4},{4,0},{8,12},{12,8},{16,20},{20,16},{24,28},{28,24},{32,36},... | collective-permute-start | bytes 1081352 | tf_op jit(solution)/shard_map/ppermute | solution.py:176
  100.1 6.1 %copy-start.23 = (bf16[4,32,1408]{2,1,0:T(8,128)(2,1)}, bf16[4,32,1408]{2,1,0:T(8,128)(2,1)S(1)}, u32[]{:S(2)}) copy-start(bf16[4,32,1408]{2,1,0:T(8,128)(2,1)S(1)} %collective-permute-done.9.refs_4_) | copy-start | bytes 1081348
  100.1 6.0 %collective-permute-start.14 = (bf16[4,32,1408]{2,1,0:T(8,128)(2,1)S(1)}, bf16[4,32,1408]{2,1,0:T(8,128)(2,1)}, u32[]{:S(2)}, u32[]{:S(2)}) collective-permute-start(bf16[4,32,1408]{2,1,0:T(8,128)(2,1)S(1)} %collective-permute-done.9.refs_4_), channel_id=1, source_target_pairs={{0,4},{4,0},{8,12},{12,8},{16,20},{20,16},{24,28},{28,24},{32,36},... | collective-permute-start | bytes 1081352 | tf_op jit(solution)/shard_map/ppermute | solution.py:176
  100.1 3.6 %copy-start.21 = (bf16[4,32,1408]{2,1,0:T(8,128)(2,1)}, bf16[4,32,1408]{2,1,0:T(8,128)(2,1)S(1)}, u32[]{:S(2)}) copy-start(bf16[4,32,1408]{2,1,0:T(8,128)(2,1)S(1)} %collective-permute-done.12.refs_10_) | copy-start | bytes 1081348
  100.1 21.8 %collective-permute-start.28 = (bf16[4,32,1408]{2,1,0:T(8,128)(2,1)}, bf16[4,32,1408]{2,1,0:T(8,128)(2,1)}, u32[]{:S(2)}, u32[]{:S(2)}) collective-permute-start(bf16[4,32,1408]{2,1,0:T(8,128)(2,1)} %get-tuple-element.30), channel_id=1, source_target_pairs={{0,8},{4,12},{8,16},{12,20},{16,24},{20,28},{24,0},{28,4},{32,40},... | collective-permute-start | bytes 1081352 | tf_op jit(solution)/shard_map/ppermute | solution.py:176
  100.2 3.5 %copy-start.22 = (bf16[4,32,1408]{2,1,0:T(8,128)(2,1)}, bf16[4,32,1408]{2,1,0:T(8,128)(2,1)S(1)}, u32[]{:S(2)}) copy-start(bf16[4,32,1408]{2,1,0:T(8,128)(2,1)S(1)} %collective-permute-done.16.refs_14_) | copy-start | bytes 1081348
  100.3 21.6 %collective-permute-start.29 = (bf16[4,32,1408]{2,1,0:T(8,128)(2,1)}, bf16[4,32,1408]{2,1,0:T(8,128)(2,1)}, u32[]{:S(2)}, u32[]{:S(2)}) collective-permute-start(bf16[4,32,1408]{2,1,0:T(8,128)(2,1)} %get-tuple-element.31), channel_id=1, source_target_pairs={{0,24},{4,28},{8,0},{12,4},{16,8},{20,12},{24,16},{28,20},{32,56},... | collective-permute-start | bytes 1081352 | tf_op jit(solution)/shard_map/ppermute | solution.py:176
  106.1 0.7 copy-start.25
  106.1 0.9 copy-start.24
  107.0 19.1 %copy-start.5 = (bf16[640,1408]{1,0:T(8,128)(2,1)S(1)}, bf16[640,1408]{1,0:T(8,128)(2,1)}, u32[]{:S(2)}) copy-start(bf16[640,1408]{1,0:T(8,128)(2,1)} %param.10) | copy-start | bytes 5406724
  118.6 32.0 %collective-permute-start.20 = (bf16[160,2048]{1,0:T(8,128)(2,1)}, bf16[160,2048]{1,0:T(8,128)(2,1)S(1)}, u32[]{:S(2)}, u32[]{:S(2)}) collective-permute-start(bf16[160,2048]{1,0:T(8,128)(2,1)} %get-tuple-element.16), channel_id=1, source_target_pairs={{0,3},{1,0},{2,1},{3,2},{4,7},{5,4},{6,5},{7,6},{8,11},{9,8},{10,9... | collective-permute-start | bytes 1966088 | tf_op jit(solution)/shard_map/ppermute | solution.py:180
  118.7 33.0 %collective-permute-start.19 = (bf16[160,2048]{1,0:T(8,128)(2,1)}, bf16[160,2048]{1,0:T(8,128)(2,1)S(1)}, u32[]{:S(2)}, u32[]{:S(2)}) collective-permute-start(bf16[160,2048]{1,0:T(8,128)(2,1)} %get-tuple-element.15), channel_id=1, source_target_pairs={{0,1},{1,2},{2,3},{3,0},{4,5},{5,6},{6,7},{7,4},{8,9},{9,10},{10,1... | collective-permute-start | bytes 1966088 | tf_op jit(solution)/shard_map/ppermute | solution.py:180
  121.9 31.7 %collective-permute-start.18 = (bf16[160,2048]{1,0:T(8,128)(2,1)}, bf16[160,2048]{1,0:T(8,128)(2,1)S(1)}, u32[]{:S(2)}, u32[]{:S(2)}) collective-permute-start(bf16[160,2048]{1,0:T(8,128)(2,1)} %get-tuple-element.14), channel_id=1, source_target_pairs={{0,2},{1,3},{2,0},{3,1},{4,6},{5,7},{6,4},{7,5},{8,10},{9,11},{10,... | collective-permute-start | bytes 1966088 | tf_op jit(solution)/shard_map/ppermute | solution.py:180
  121.9 4.2 %copy-start.1 = (bf16[4,160,2048]{2,1,0:T(8,128)(2,1)S(1)}, bf16[4,160,2048]{2,1,0:T(8,128)(2,1)}, u32[]{:S(2)}) copy-start(bf16[4,160,2048]{2,1,0:T(8,128)(2,1)} %copy-done) | copy-start | bytes 7864324
  121.9 4.2 %copy-start.4 = (bf16[640,1408]{1,0:T(8,128)(2,1)S(1)}, bf16[640,1408]{1,0:T(8,128)(2,1)}, u32[]{:S(2)}) copy-start(bf16[640,1408]{1,0:T(8,128)(2,1)} %param.9) | copy-start | bytes 5406724
  123.7 32.4 %collective-permute-start.36 = (bf16[32,1408]{1,0:T(8,128)(2,1)S(1)}, bf16[32,1408]{1,0:T(8,128)(2,1)S(1)}, u32[]{:S(2)}, u32[]{:S(2)}) collective-permute-start(bf16[32,1408]{1,0:T(8,128)(2,1)S(1)} %fusion.52), channel_id=1, source_target_pairs={{0,224},{4,228},{8,232},{12,236},{16,240},{20,244},{24,248},{28,25... | collective-permute-start | bytes 270344 | tf_op jit(solution)/shard_map/ppermute | solution.py:176
  125.4 32.1 %collective-permute-start.35 = (bf16[32,1408]{1,0:T(8,128)(2,1)S(1)}, bf16[32,1408]{1,0:T(8,128)(2,1)S(1)}, u32[]{:S(2)}, u32[]{:S(2)}) collective-permute-start(bf16[32,1408]{1,0:T(8,128)(2,1)S(1)} %get-tuple-element.37), channel_id=1, source_target_pairs={{0,32},{4,36},{8,40},{12,44},{16,48},{20,52},{24,56},{28,60},{32,6... | collective-permute-start | bytes 270344 | tf_op jit(solution)/shard_map/ppermute | solution.py:176
  126.1 35.5 %copy-start.8 = (bf16[160,2048]{1,0:T(8,128)(2,1)S(1)}, bf16[160,2048]{1,0:T(8,128)(2,1)}, u32[]{:S(2)}) copy-start(bf16[160,2048]{1,0:T(8,128)(2,1)} %get-tuple-element.13) | copy-start | bytes 1966084
  135.4 35.2 %copy-start.10 = (f32[1408,32]{0,1:T(8,128)S(1)}, f32[1408,32]{0,1:T(8,128)}, u32[]{:S(2)}) copy-start(f32[1408,32]{0,1:T(8,128)} %param.13) | copy-start | bytes 540676
  150.6 12.4 %collective-permute-start.34 = (bf16[32,1408]{1,0:T(8,128)(2,1)S(1)}, bf16[32,1408]{1,0:T(8,128)(2,1)S(1)}, u32[]{:S(2)}, u32[]{:S(2)}) collective-permute-start(bf16[32,1408]{1,0:T(8,128)(2,1)S(1)} %get-tuple-element.36), channel_id=1, source_target_pairs={{0,192},{4,196},{8,200},{12,204},{16,208},{20,212},{24,216},{28,22... | collective-permute-start | bytes 270344 | tf_op jit(solution)/shard_map/ppermute | solution.py:176
  151.7 11.4 %collective-permute-start.33 = (bf16[32,1408]{1,0:T(8,128)(2,1)S(1)}, bf16[32,1408]{1,0:T(8,128)(2,1)S(1)}, u32[]{:S(2)}, u32[]{:S(2)}) collective-permute-start(bf16[32,1408]{1,0:T(8,128)(2,1)S(1)} %get-tuple-element.35), channel_id=1, source_target_pairs={{0,64},{4,68},{8,72},{12,76},{16,80},{20,84},{24,88},{28,92},{32,9... | collective-permute-start | bytes 270344 | tf_op jit(solution)/shard_map/ppermute | solution.py:176
  153.5 9.5 %collective-permute-start.32 = (bf16[32,1408]{1,0:T(8,128)(2,1)S(1)}, bf16[32,1408]{1,0:T(8,128)(2,1)S(1)}, u32[]{:S(2)}, u32[]{:S(2)}) collective-permute-start(bf16[32,1408]{1,0:T(8,128)(2,1)S(1)} %get-tuple-element.34), channel_id=1, source_target_pairs={{0,160},{4,164},{8,168},{12,172},{16,176},{20,180},{24,184},{28,18... | collective-permute-start | bytes 270344 | tf_op jit(solution)/shard_map/ppermute | solution.py:176
  156.1 11.1 %collective-permute-start.31 = (bf16[32,1408]{1,0:T(8,128)(2,1)S(1)}, bf16[32,1408]{1,0:T(8,128)(2,1)S(1)}, u32[]{:S(2)}, u32[]{:S(2)}) collective-permute-start(bf16[32,1408]{1,0:T(8,128)(2,1)S(1)} %get-tuple-element.33), channel_id=1, source_target_pairs={{0,96},{4,100},{8,104},{12,108},{16,112},{20,116},{24,120},{28,124... | collective-permute-start | bytes 270344 | tf_op jit(solution)/shard_map/ppermute | solution.py:176
  157.5 13.0 %collective-permute-start.30 = (bf16[32,1408]{1,0:T(8,128)(2,1)S(1)}, bf16[32,1408]{1,0:T(8,128)(2,1)S(1)}, u32[]{:S(2)}, u32[]{:S(2)}) collective-permute-start(bf16[32,1408]{1,0:T(8,128)(2,1)S(1)} %get-tuple-element.32), channel_id=1, source_target_pairs={{0,128},{4,132},{8,136},{12,140},{16,144},{20,148},{24,152},{28,15... | collective-permute-start | bytes 270344 | tf_op jit(solution)/shard_map/ppermute | solution.py:176

commit v2 on v1

--- a/solution.py
+++ b/solution.py
@@ -59,7 +59,9 @@
             jax.ShapeDtypeStruct((NY, NZ, w, ff), BF),
             jax.ShapeDtypeStruct((NY, NZ, w, ff), BF),
         ],
-        compiler_params=pltpu.CompilerParams(dimension_semantics=("arbitrary",)),
+        compiler_params=pltpu.CompilerParams(
+            dimension_semantics=("arbitrary",), vmem_limit_bytes=24 * 1024 * 1024
+        ),
         cost_estimate=pl.CostEstimate(
             flops=2 * n * d * ff, bytes_accessed=12 * 1024 * 1024, transcendentals=0
         ),
@@ -152,7 +154,9 @@
         ),
         out_shape=[jax.ShapeDtypeStruct((rows, d), BF)] * parts
         + [jax.ShapeDtypeStruct((count, NY, NC, w, ff), BF)],
-        compiler_params=pltpu.CompilerParams(dimension_semantics=("arbitrary",)),
+        compiler_params=pltpu.CompilerParams(
+            dimension_semantics=("arbitrary",), vmem_limit_bytes=24 * 1024 * 1024
+        ),
         cost_estimate=pl.CostEstimate(
             flops=2 * parts * rows * d * ff,
             bytes_accessed=16 * 1024 * 1024,

time: 172 us -> 180 us (1.047)
  local copies, waits for them, and re-layouts: 6.16 us -> 17.1 us
  matrix products: 9.23 us -> 6.41 us
  waiting for transfers between devices: 68.4 us -> 70.6 us
    unnamed x52 -> x60, local copies, waits for them, and re-layouts: 2.44 us -> 12.4 us
    dot_general x1, matrix products: 9.23 us -> 6.41 us  [step(): jnp.dot(cot_rows, whole.reshape(d, ff), preferred_element_type=F32)]
    ppermute x7, waiting for transfers between devices: 30.9 us -> 33.6 us  [shift_x(): return lax.ppermute(x, 'tp', [(i, (i + d) % NX) for i in range(NX)])]
    pallas_call x1, Pallas kernels: 9.52 us -> 7 us  [grad_term(): pl.pallas_call(body, grid_spec=pltpu.PrefetchScalarGridSpec(num_scalar_pr...]
    pallas_call x1, Pallas kernels: 11.6 us -> 13.9 us  [partial_products(): pl.pallas_call(body, grid_spec=pltpu.PrefetchScalarGridSpec(num_scalar_pr...]
  transfers between devices with their start and end apart: 37 -> 37, of which waited for: 14 -> 14; matrix products, arithmetic and copies ran while one was open for 16% -> 13% of each run, Pallas kernels for 7% -> 8%
where the time goes in v2:
time: 180 us
  waiting for transfers between devices  70.6 us (39%)
  starting transfers between devices  49.9 us (28%)
  Pallas kernels  20.9 us (12%)
  local copies, waits for them, and re-layouts  17.1 us (10%)
  other arithmetic  13.7 us (8%)
  matrix products  6.41 us (4%)
    ppermute x30, starting transfers between devices, shift(): return lax.ppermute(x, 'fs', perm)  39.5 us
    ppermute x30, waiting for transfers between devices, shift(): return lax.ppermute(x, 'fs', perm)  37.1 us
    ppermute x7, waiting for transfers between devices, shift_x(): return lax.ppermute(x, 'tp', [(i, (i + d) % NX) for i in range(NX)])  33.6 us
    pallas_call x1, Pallas kernels, partial_products(): pl.pallas_call(body, grid_spec=pltpu.PrefetchScalarGridSpec(num_scalar_pr...  13.9 us
    unnamed x60, local copies, waits for them, and re-layouts  12.4 us
    ppermute x7, starting transfers between devices, shift_x(): return lax.ppermute(x, 'tp', [(i, (i + d) % NX) for i in range(NX)])  10.4 us
    pallas_call x1, Pallas kernels, grad_term(): pl.pallas_call(body, grid_spec=pltpu.PrefetchScalarGridSpec(num_scalar_pr...  7 us
    dot_general x1, matrix products, step(): jnp.dot(cot_rows, whole.reshape(d, ff), preferred_element_type=F32)  6.41 us
  transfers between devices with their start and end apart: 37, of which 14 were waited for; matrix products, arithmetic and copies ran while one was open for 13% of the time, Pallas kernels for 8%

profile of v2, /device:TPU:6, one launch (start us, length us, event | category | flops | bytes accessed | tf_op | source)
XLA Modules:
  0.0 179.5 jit_solution(13085888085608395718)
XLA Ops:
  0.6 0.9 collective-permute-start.21
  1.5 2.4 %collective-permute-start.22 = (bf16[160,2048]{1,0:T(8,128)(2,1)}, bf16[160,2048]{1,0:T(8,128)(2,1)}, u32[]{:S(2)}, u32[]{:S(2)}) collective-permute-start(bf16[160,2048]{1,0:T(8,128)(2,1)} %param.11), channel_id=1, source_target_pairs={{0,1},{1,2},{2,3},{3,0},{4,5},{5,6},{6,7},{7,4},{8,9},{9,10},{10,1... | collective-permute-start | bytes 1966088 | tf_op jit(solution)/shard_map/ppermute | solution.py:184
  3.9 4.3 %fusion.16.hidden = bf16[640,1408]{1,0:T(8,128)(2,1)} fusion(bf16[640,1408]{1,0:T(8,128)(2,1)} %param.10, bf16[640,1408]{1,0:T(8,128)(2,1)} %param.9), kind=kLoop, calls=%fused_computation.23 | loop fusion | flops 7208960 | bytes 5406720 | tf_op jit(solution)/shard_map/convert_element_type | solution.py:220
  8.4 0.3 broadcast_in_dim.18
  8.7 0.7 copy-done.27
  9.5 8.6 %collective-permute-done.22 = bf16[160,2048]{1,0:T(8,128)(2,1)} collective-permute-done((bf16[160,2048]{1,0:T(8,128)(2,1)}, bf16[160,2048]{1,0:T(8,128)(2,1)}, u32[]{:S(2)}, u32[]{:S(2)}) %collective-permute-start.22) | collective-permute-done | bytes 655392 | tf_op jit(solution)/shard_map/ppermute | solution.py:184
  18.0 1.0 slice.88
  19.0 3.7 %collective-permute-start.23 = (bf16[80,2048]{1,0:T(8,128)(2,1)S(1)}, bf16[80,2048]{1,0:T(8,128)(2,1)S(1)}, u32[]{:S(2)}, u32[]{:S(2)}) collective-permute-start(bf16[80,2048]{1,0:T(8,128)(2,1)S(1)} %slice.88), channel_id=1, source_target_pairs={{0,1},{1,2},{2,3},{3,0},{4,5},{5,6},{6,7},{7,4},{8,9},{9,10},{10,1... | collective-permute-start | bytes 983048 | tf_op jit(solution)/shard_map/ppermute | solution.py:184
  22.7 1.0 slice.89
  23.8 1.1 bitcast_dynamic-update-slice_fusion.1
  25.0 1.1 bitcast_dynamic-update-slice_fusion
  26.1 2.4 %collective-permute-done.23 = bf16[80,2048]{1,0:T(8,128)(2,1)S(1)} collective-permute-done((bf16[80,2048]{1,0:T(8,128)(2,1)S(1)}, bf16[80,2048]{1,0:T(8,128)(2,1)S(1)}, u32[]{:S(2)}, u32[]{:S(2)}) %collective-permute-start.23) | collective-permute-done | bytes 327712 | tf_op jit(solution)/shard_map/ppermute | solution.py:184
  28.6 4.5 %collective-permute-done.24 = bf16[80,2048]{1,0:T(8,128)(2,1)S(1)} collective-permute-done((bf16[80,2048]{1,0:T(8,128)(2,1)S(1)}, bf16[80,2048]{1,0:T(8,128)(2,1)S(1)}, u32[]{:S(2)}, u32[]{:S(2)}) %collective-permute-start.24) | collective-permute-done | bytes 327712 | tf_op jit(solution)/shard_map/ppermute | solution.py:184
  33.1 7.0 %grad_term.1 = (bf16[4,8,32,1408]{3,2,1,0:T(8,128)(2,1)S(1)}, bf16[4,8,32,1408]{3,2,1,0:T(8,128)(2,1)S(1)}) custom-call(s32[4]{0:T(128)S(1)} %pad_add_fusion.where, bf16[640,2048]{1,0:T(8,128)(2,1)S(1)} %bitcast.78, bf16[640,1408]{1,0:T(8,128)(2,1)S(1)} %copy-done.1), custom_call_target="tpu_custom_call" | custom-call | flops 3690987520 | bytes 12582912 | tf_op jit(solution)/shard_map/grad_term/pallas_call | solution.py:44
  40.2 1.6 collective-permute-start.2
  41.9 2.9 %collective-permute-start.1 = (bf16[32,1408]{1,0:T(8,128)(2,1)S(1)}, bf16[32,1408]{1,0:T(8,128)(2,1)S(1)}, u32[]{:S(2)}, u32[]{:S(2)}) collective-permute-start(bf16[32,1408]{1,0:T(8,128)(2,1)S(1)} %bitcast.83), channel_id=1, source_target_pairs={{0,16},{4,20},{8,24},{12,28},{16,0},{20,4},{24,8},{28,12},{32,48},... | collective-permute-start | bytes 270344 | tf_op jit(solution)/shard_map/ppermute | solution.py:180
  44.8 1.3 collective-permute-start
  46.1 0.4 collective-permute-done.2
  46.5 3.1 %collective-permute-done.1 = bf16[32,1408]{1,0:T(8,128)(2,1)S(1)} collective-permute-done((bf16[32,1408]{1,0:T(8,128)(2,1)S(1)}, bf16[32,1408]{1,0:T(8,128)(2,1)S(1)}, u32[]{:S(2)}, u32[]{:S(2)}) %collective-permute-start.1) | collective-permute-done | bytes 90144 | tf_op jit(solution)/shard_map/ppermute | solution.py:180
  49.7 2.0 %collective-permute-start.6 = (bf16[4,32,1408]{2,1,0:T(8,128)(2,1)S(1)}, bf16[4,32,1408]{2,1,0:T(8,128)(2,1)S(1)}, u32[]{:S(2)}, u32[]{:S(2)}) collective-permute-start(bf16[4,32,1408]{2,1,0:T(8,128)(2,1)S(1)} %pad_maximum_fusion.refs_0_), channel_id=1, source_target_pairs={{0,32},{4,36},{8,40},{12,44},{16,48},{20,52},{24,56},{28,60},{32,6... | collective-permute-start | bytes 1081352 | tf_op jit(solution)/shard_map/ppermute | solution.py:180
  51.7 4.0 %collective-permute-start.3 = (bf16[4,32,1408]{2,1,0:T(8,128)(2,1)S(1)}, bf16[4,32,1408]{2,1,0:T(8,128)(2,1)S(1)}, u32[]{:S(2)}, u32[]{:S(2)}) collective-permute-start(bf16[4,32,1408]{2,1,0:T(8,128)(2,1)S(1)} %pad_maximum_fusion.refs_0_), channel_id=1, source_target_pairs={{0,224},{4,228},{8,232},{12,236},{16,240},{20,244},{24,248},{28,25... | collective-permute-start | bytes 1081352 | tf_op jit(solution)/shard_map/ppermute | solution.py:180
  55.7 8.0 %collective-permute-done.6.refs_7_ = bf16[4,32,1408]{2,1,0:T(8,128)(2,1)S(1)} collective-permute-done((bf16[4,32,1408]{2,1,0:T(8,128)(2,1)S(1)}, bf16[4,32,1408]{2,1,0:T(8,128)(2,1)S(1)}, u32[]{:S(2)}, u32[]{:S(2)}) %collective-permute-start.6) | collective-permute-done | bytes 360480 | tf_op jit(solution)/shard_map/ppermute | solution.py:180
  63.8 1.8 fusion.19
  65.8 3.0 %collective-permute-start.26 = (bf16[8,32,1408]{2,1,0:T(8,128)(2,1)S(1)}, bf16[8,32,1408]{2,1,0:T(8,128)(2,1)S(1)}, u32[]{:S(2)}, u32[]{:S(2)}) collective-permute-start(bf16[8,32,1408]{2,1,0:T(8,128)(2,1)S(1)} %get-tuple-element.24), channel_id=1, source_target_pairs={{0,24},{4,28},{8,0},{12,4},{16,8},{20,12},{24,16},{28,20},{32,56},... | collective-permute-start | bytes 2162696 | tf_op jit(solution)/shard_map/ppermute | solution.py:180
  68.8 3.2 %collective-permute-start.4 = (bf16[4,32,1408]{2,1,0:T(8,128)(2,1)S(1)}, bf16[4,32,1408]{2,1,0:T(8,128)(2,1)S(1)}, u32[]{:S(2)}, u32[]{:S(2)}) collective-permute-start(bf16[4,32,1408]{2,1,0:T(8,128)(2,1)S(1)} %collective-permute-done.3.refs_1_), channel_id=1, source_target_pairs={{0,224},{4,228},{8,232},{12,236},{16,240},{20,244},{24,248},{28,25... | collective-permute-start | bytes 1081352 | tf_op jit(solution)/shard_map/ppermute | solution.py:180
  72.0 2.2 %collective-permute-done.7.refs_6_ = bf16[4,32,1408]{2,1,0:T(8,128)(2,1)S(1)} collective-permute-done((bf16[4,32,1408]{2,1,0:T(8,128)(2,1)S(1)}, bf16[4,32,1408]{2,1,0:T(8,128)(2,1)S(1)}, u32[]{:S(2)}, u32[]{:S(2)}) %collective-permute-start.7) | collective-permute-done | bytes 360480 | tf_op jit(solution)/shard_map/ppermute | solution.py:180
  74.3 3.7 %collective-permute-done.4.refs_2_ = bf16[4,32,1408]{2,1,0:T(8,128)(2,1)S(1)} collective-permute-done((bf16[4,32,1408]{2,1,0:T(8,128)(2,1)S(1)}, bf16[4,32,1408]{2,1,0:T(8,128)(2,1)S(1)}, u32[]{:S(2)}, u32[]{:S(2)}) %collective-permute-start.4) | collective-permute-done | bytes 360480 | tf_op jit(solution)/shard_map/ppermute | solution.py:180
  78.0 3.8 %collective-permute-start.5 = (bf16[4,32,1408]{2,1,0:T(8,128)(2,1)S(1)}, bf16[4,32,1408]{2,1,0:T(8,128)(2,1)}, u32[]{:S(2)}, u32[]{:S(2)}) collective-permute-start(bf16[4,32,1408]{2,1,0:T(8,128)(2,1)S(1)} %collective-permute-done.4.refs_2_), channel_id=1, source_target_pairs={{0,224},{4,228},{8,232},{12,236},{16,240},{20,244},{24,248},{28,25... | collective-permute-start | bytes 1081352 | tf_op jit(solution)/shard_map/ppermute | solution.py:180
  81.8 2.4 %collective-permute-done.8.refs_5_ = bf16[4,32,1408]{2,1,0:T(8,128)(2,1)} collective-permute-done((bf16[4,32,1408]{2,1,0:T(8,128)(2,1)S(1)}, bf16[4,32,1408]{2,1,0:T(8,128)(2,1)}, u32[]{:S(2)}, u32[]{:S(2)}) %collective-permute-start.8) | collective-permute-done | bytes 360480 | tf_op jit(solution)/shard_map/ppermute | solution.py:180
  84.2 0.5 collective-permute-start.16
  84.7 1.1 fusion.26
  85.8 0.7 copy-done.12
  86.8 3.2 %collective-permute-done.5.refs_3_ = bf16[4,32,1408]{2,1,0:T(8,128)(2,1)} collective-permute-done((bf16[4,32,1408]{2,1,0:T(8,128)(2,1)S(1)}, bf16[4,32,1408]{2,1,0:T(8,128)(2,1)}, u32[]{:S(2)}, u32[]{:S(2)}) %collective-permute-start.5) | collective-permute-done | bytes 360480 | tf_op jit(solution)/shard_map/ppermute | solution.py:180
  90.1 6.6 %collective-permute-done.9.refs_4_ = bf16[4,32,1408]{2,1,0:T(8,128)(2,1)} collective-permute-done((bf16[4,32,1408]{2,1,0:T(8,128)(2,1)}, bf16[4,32,1408]{2,1,0:T(8,128)(2,1)}, u32[]{:S(2)}, u32[]{:S(2)}) %collective-permute-start.9) | collective-permute-done | bytes 360480 | tf_op jit(solution)/shard_map/ppermute | solution.py:180
  96.7 0.8 copy-done.14
  97.4 0.8 copy-done.16
  98.2 3.2 %collective-permute-start.29 = (bf16[4,32,1408]{2,1,0:T(8,128)(2,1)}, bf16[4,32,1408]{2,1,0:T(8,128)(2,1)}, u32[]{:S(2)}, u32[]{:S(2)}) collective-permute-start(bf16[4,32,1408]{2,1,0:T(8,128)(2,1)} %get-tuple-element.31), channel_id=1, source_target_pairs={{0,24},{4,28},{8,0},{12,4},{16,8},{20,12},{24,16},{28,20},{32,56},... | collective-permute-start | bytes 1081352 | tf_op jit(solution)/shard_map/ppermute | solution.py:180
  101.5 2.3 %fusion.17 = bf16[640,1408]{1,0:T(8,128)(2,1)} fusion(bf16[640,1408]{1,0:T(8,128)(2,1)S(1)} %copy-done.19, bf16[640,1408]{1,0:T(8,128)(2,1)S(1)} %copy-done.20), kind=kLoop, calls=%fused_computation.24 | loop fusion | flops 7208960 | bytes 5406720 | tf_op jit(solution)/shard_map/convert_element_type | solution.py:215
  103.8 1.5 copy-done
  105.3 1.0 copy-done.3
  106.3 1.0 copy-done.5
  107.3 1.0 copy-done.7
  108.2 1.0 copy-done.9
  109.2 1.0 copy-done.11
  110.2 1.0 copy-done.13
  111.2 1.0 copy-done.15
  112.2 1.0 copy-done.17
  113.2 13.9 %partial_products.1 = (bf16[160,2048]{1,0:T(8,128)(2,1)S(1)}, bf16[160,2048]{1,0:T(8,128)(2,1)S(1)}, bf16[160,2048]{1,0:T(8,128)(2,1)S(1)}, bf16[160,2048]{1,0:T...) custom-call(s32[4]{0:T(128)S(1)} %pad_add_fusion.where, bf16[4,160,1408]{2,1,0:T(8,128)(2,1)S(1)} %bitcast.80, ...), custom_call_target="tpu_custom_call" | custom-call | flops 3690987520 | bytes 16777216 | tf_op jit(solution)/shard_map/partial_products/pallas_call | solution.py:135
  127.2 3.2 %collective-permute-start.19 = (bf16[160,2048]{1,0:T(8,128)(2,1)S(1)}, bf16[160,2048]{1,0:T(8,128)(2,1)S(1)}, u32[]{:S(2)}, u32[]{:S(2)}) collective-permute-start(bf16[160,2048]{1,0:T(8,128)(2,1)S(1)} %get-tuple-element.15), channel_id=1, source_target_pairs={{0,1},{1,2},{2,3},{3,0},{4,5},{5,6},{6,7},{7,4},{8,9},{9,10},{10,1... | collective-permute-start | bytes 1966088 | tf_op jit(solution)/shard_map/ppermute | solution.py:184
  130.5 1.5 fusion.29
  132.1 1.3 collective-permute-start.36
  133.4 0.3 fusion.51
  133.7 0.9 collective-permute-start.35
  134.5 6.4 %fusion.15 = (bf16[640,1408]{1,0:T(8,128)(2,1)}, bf16[640,1408]{1,0:T(8,128)(2,1)}) fusion(bf16[640,1408]{1,0:T(8,128)(2,1)S(1)} %copy-done.21, bf16[640,1408]{1,0:T(8,128)(2,1)S(1)} %copy-done.22, bf16[640,2048]{1,0:T(8,128)(2,1)S(1)} %bitcast.79, bf16[2048,1408]{1,0:T(8,128)(2,1)S(1)} %bitcast.81), kind=kOutput, calls=%fused_computation.22 | convolution fusion | flops 3704504320 | bytes 15597568 | tf_op jit(solution)/shard_map/dot_general | solution.py:267
  140.9 18.1 %collective-permute-done.20 = bf16[160,2048]{1,0:T(8,128)(2,1)S(1)} collective-permute-done((bf16[160,2048]{1,0:T(8,128)(2,1)S(1)}, bf16[160,2048]{1,0:T(8,128)(2,1)S(1)}, u32[]{:S(2)}, u32[]{:S(2)}) %collective-permute-start.20) | collective-permute-done | bytes 655392 | tf_op jit(solution)/shard_map/ppermute | solution.py:184
  159.0 0.9 collective-permute-start.34
  159.9 2.0 %collective-permute-start.33 = (bf16[32,1408]{1,0:T(8,128)(2,1)S(1)}, bf16[32,1408]{1,0:T(8,128)(2,1)S(1)}, u32[]{:S(2)}, u32[]{:S(2)}) collective-permute-start(bf16[32,1408]{1,0:T(8,128)(2,1)S(1)} %get-tuple-element.35), channel_id=1, source_target_pairs={{0,64},{4,68},{8,72},{12,76},{16,80},{20,84},{24,88},{28,92},{32,9... | collective-permute-start | bytes 270344 | tf_op jit(solution)/shard_map/ppermute | solution.py:180
  161.9 2.4 %collective-permute-start.32 = (bf16[32,1408]{1,0:T(8,128)(2,1)S(1)}, bf16[32,1408]{1,0:T(8,128)(2,1)S(1)}, u32[]{:S(2)}, u32[]{:S(2)}) collective-permute-start(bf16[32,1408]{1,0:T(8,128)(2,1)S(1)} %get-tuple-element.34), channel_id=1, source_target_pairs={{0,160},{4,164},{8,168},{12,172},{16,176},{20,180},{24,184},{28,18... | collective-permute-start | bytes 270344 | tf_op jit(solution)/shard_map/ppermute | solution.py:180
  164.3 1.5 collective-permute-start.31
  165.8 4.2 %collective-permute-start.30 = (bf16[32,1408]{1,0:T(8,128)(2,1)S(1)}, bf16[32,1408]{1,0:T(8,128)(2,1)S(1)}, u32[]{:S(2)}, u32[]{:S(2)}) collective-permute-start(bf16[32,1408]{1,0:T(8,128)(2,1)S(1)} %get-tuple-element.32), channel_id=1, source_target_pairs={{0,128},{4,132},{8,136},{12,140},{16,144},{20,148},{24,152},{28,15... | collective-permute-start | bytes 270344 | tf_op jit(solution)/shard_map/ppermute | solution.py:180
  170.0 1.3 add_convert_fusion.2
  171.4 4.3 %collective-permute-done.31 = bf16[32,1408]{1,0:T(8,128)(2,1)S(1)} collective-permute-done((bf16[32,1408]{1,0:T(8,128)(2,1)S(1)}, bf16[32,1408]{1,0:T(8,128)(2,1)S(1)}, u32[]{:S(2)}, u32[]{:S(2)}) %collective-permute-start.31) | collective-permute-done | bytes 90144 | tf_op jit(solution)/shard_map/ppermute | solution.py:180
  175.7 3.0 %collective-permute-done.30 = bf16[32,1408]{1,0:T(8,128)(2,1)S(1)} collective-permute-done((bf16[32,1408]{1,0:T(8,128)(2,1)S(1)}, bf16[32,1408]{1,0:T(8,128)(2,1)S(1)}, u32[]{:S(2)}, u32[]{:S(2)}) %collective-permute-start.30) | collective-permute-done | bytes 90144 | tf_op jit(solution)/shard_map/ppermute | solution.py:180
  178.7 0.8 fusion.37
  (92 shorter events, 1.2 us)
Async XLA Ops:
  0.6 22.1 %collective-permute-start.21 = (bf16[160,2048]{1,0:T(8,128)(2,1)}, bf16[160,2048]{1,0:T(8,128)(2,1)}, u32[]{:S(2)}, u32[]{:S(2)}) collective-permute-start(bf16[160,2048]{1,0:T(8,128)(2,1)} %param.11), channel_id=1, source_target_pairs={{0,3},{1,0},{2,1},{3,2},{4,7},{5,4},{6,5},{7,6},{8,11},{9,8},{10,9... | collective-permute-start | bytes 1966088 | tf_op jit(solution)/shard_map/ppermute | solution.py:184
  1.5 16.5 %collective-permute-start.22 = (bf16[160,2048]{1,0:T(8,128)(2,1)}, bf16[160,2048]{1,0:T(8,128)(2,1)}, u32[]{:S(2)}, u32[]{:S(2)}) collective-permute-start(bf16[160,2048]{1,0:T(8,128)(2,1)} %param.11), channel_id=1, source_target_pairs={{0,1},{1,2},{2,3},{3,0},{4,5},{5,6},{6,7},{7,4},{8,9},{9,10},{10,1... | collective-permute-start | bytes 1966088 | tf_op jit(solution)/shard_map/ppermute | solution.py:184
  8.3 1.1 copy-start.27
  9.4 23.7 %copy-start.1 = (bf16[640,1408]{1,0:T(8,128)(2,1)S(1)}, bf16[640,1408]{1,0:T(8,128)(2,1)}, u32[]{:S(2)}) copy-start(bf16[640,1408]{1,0:T(8,128)(2,1)} %fusion.16.hidden) | copy-start | bytes 5406724
  19.0 9.5 %collective-permute-start.23 = (bf16[80,2048]{1,0:T(8,128)(2,1)S(1)}, bf16[80,2048]{1,0:T(8,128)(2,1)S(1)}, u32[]{:S(2)}, u32[]{:S(2)}) collective-permute-start(bf16[80,2048]{1,0:T(8,128)(2,1)S(1)} %slice.88), channel_id=1, source_target_pairs={{0,1},{1,2},{2,3},{3,0},{4,5},{5,6},{6,7},{7,4},{8,9},{9,10},{10,1... | collective-permute-start | bytes 983048 | tf_op jit(solution)/shard_map/ppermute | solution.py:184
  23.7 9.3 %collective-permute-start.24 = (bf16[80,2048]{1,0:T(8,128)(2,1)S(1)}, bf16[80,2048]{1,0:T(8,128)(2,1)S(1)}, u32[]{:S(2)}, u32[]{:S(2)}) collective-permute-start(bf16[80,2048]{1,0:T(8,128)(2,1)S(1)} %slice.89), channel_id=1, source_target_pairs={{0,3},{1,0},{2,1},{3,2},{4,7},{5,4},{6,5},{7,6},{8,11},{9,8},{10,9... | collective-permute-start | bytes 983048 | tf_op jit(solution)/shard_map/ppermute | solution.py:184
  33.1 7.1 %copy-start.29 = (bf16[1408,32]{0,1:T(8,128)(2,1)S(1)}, bf16[1408,32]{0,1:T(8,128)(2,1)}, u32[]{:S(2)}) copy-start(bf16[1408,32]{0,1:T(8,128)(2,1)} %param.12) | copy-start | bytes 270340
  40.1 23.6 %collective-permute-start.25 = (bf16[4,8,32,1408]{3,2,1,0:T(8,128)(2,1)S(1)}, bf16[4,8,32,1408]{3,2,1,0:T(8,128)(2,1)S(1)}, u32[]{:S(2)}, u32[]{:S(2)}) collective-permute-start(bf16[4,8,32,1408]{3,2,1,0:T(8,128)(2,1)S(1)} %get-tuple-element.21), channel_id=1, source_target_pairs={{0,4},{4,0},{8,12},{12,8},{16,20},{20,16},{24,28},{28,24},{32,36},... | collective-permute-start | bytes 8650760 | tf_op jit(solution)/shard_map/ppermute | solution.py:180
  40.2 6.3 %collective-permute-start.2 = (bf16[32,1408]{1,0:T(8,128)(2,1)S(1)}, bf16[32,1408]{1,0:T(8,128)(2,1)S(1)}, u32[]{:S(2)}, u32[]{:S(2)}) collective-permute-start(bf16[32,1408]{1,0:T(8,128)(2,1)S(1)} %bitcast.82), channel_id=1, source_target_pairs={{0,8},{4,12},{8,16},{12,20},{16,24},{20,28},{24,0},{28,4},{32,40},... | collective-permute-start | bytes 270344 | tf_op jit(solution)/shard_map/ppermute | solution.py:180
  41.9 7.7 %collective-permute-start.1 = (bf16[32,1408]{1,0:T(8,128)(2,1)S(1)}, bf16[32,1408]{1,0:T(8,128)(2,1)S(1)}, u32[]{:S(2)}, u32[]{:S(2)}) collective-permute-start(bf16[32,1408]{1,0:T(8,128)(2,1)S(1)} %bitcast.83), channel_id=1, source_target_pairs={{0,16},{4,20},{8,24},{12,28},{16,0},{20,4},{24,8},{28,12},{32,48},... | collective-permute-start | bytes 270344 | tf_op jit(solution)/shard_map/ppermute | solution.py:180
  44.8 4.8 %collective-permute-start = (bf16[32,1408]{1,0:T(8,128)(2,1)S(1)}, bf16[32,1408]{1,0:T(8,128)(2,1)S(1)}, u32[]{:S(2)}, u32[]{:S(2)}) collective-permute-start(bf16[32,1408]{1,0:T(8,128)(2,1)S(1)} %bitcast.84), channel_id=1, source_target_pairs={{0,24},{4,28},{8,0},{12,4},{16,8},{20,12},{24,16},{28,20},{32,56},... | collective-permute-start | bytes 270344 | tf_op jit(solution)/shard_map/ppermute | solution.py:180
  49.7 14.1 %collective-permute-start.6 = (bf16[4,32,1408]{2,1,0:T(8,128)(2,1)S(1)}, bf16[4,32,1408]{2,1,0:T(8,128)(2,1)S(1)}, u32[]{:S(2)}, u32[]{:S(2)}) collective-permute-start(bf16[4,32,1408]{2,1,0:T(8,128)(2,1)S(1)} %pad_maximum_fusion.refs_0_), channel_id=1, source_target_pairs={{0,32},{4,36},{8,40},{12,44},{16,48},{20,52},{24,56},{28,60},{32,6... | collective-permute-start | bytes 1081352 | tf_op jit(solution)/shard_map/ppermute | solution.py:180
  51.7 17.1 %collective-permute-start.3 = (bf16[4,32,1408]{2,1,0:T(8,128)(2,1)S(1)}, bf16[4,32,1408]{2,1,0:T(8,128)(2,1)S(1)}, u32[]{:S(2)}, u32[]{:S(2)}) collective-permute-start(bf16[4,32,1408]{2,1,0:T(8,128)(2,1)S(1)} %pad_maximum_fusion.refs_0_), channel_id=1, source_target_pairs={{0,224},{4,228},{8,232},{12,236},{16,240},{20,244},{24,248},{28,25... | collective-permute-start | bytes 1081352 | tf_op jit(solution)/shard_map/ppermute | solution.py:180
  55.7 16.3 %collective-permute-start.10 = (bf16[4,32,1408]{2,1,0:T(8,128)(2,1)S(1)}, bf16[4,32,1408]{2,1,0:T(8,128)(2,1)S(1)}, u32[]{:S(2)}, u32[]{:S(2)}) collective-permute-start(bf16[4,32,1408]{2,1,0:T(8,128)(2,1)S(1)} %pad_maximum_fusion.refs_0_), channel_id=1, source_target_pairs={{0,4},{4,0},{8,12},{12,8},{16,20},{20,16},{24,28},{28,24},{32,36},... | collective-permute-start | bytes 1081352 | tf_op jit(solution)/shard_map/ppermute | solution.py:180
  63.7 10.5 %collective-permute-start.7 = (bf16[4,32,1408]{2,1,0:T(8,128)(2,1)S(1)}, bf16[4,32,1408]{2,1,0:T(8,128)(2,1)S(1)}, u32[]{:S(2)}, u32[]{:S(2)}) collective-permute-start(bf16[4,32,1408]{2,1,0:T(8,128)(2,1)S(1)} %collective-permute-done.6.refs_7_), channel_id=1, source_target_pairs={{0,32},{4,36},{8,40},{12,44},{16,48},{20,52},{24,56},{28,60},{32,6... | collective-permute-start | bytes 1081352 | tf_op jit(solution)/shard_map/ppermute | solution.py:180
  63.8 37.7 %copy-start.20 = (bf16[640,1408]{1,0:T(8,128)(2,1)S(1)}, bf16[640,1408]{1,0:T(8,128)(2,1)}, u32[]{:S(2)}) copy-start(bf16[640,1408]{1,0:T(8,128)(2,1)} %param.7) | copy-start | bytes 5406724
  65.6 35.9 %copy-start.19 = (bf16[640,1408]{1,0:T(8,128)(2,1)S(1)}, bf16[640,1408]{1,0:T(8,128)(2,1)}, u32[]{:S(2)}) copy-start(bf16[640,1408]{1,0:T(8,128)(2,1)} %param.8) | copy-start | bytes 5406724
  65.6 18.6 %collective-permute-start.27 = (bf16[8,32,1408]{2,1,0:T(8,128)(2,1)S(1)}, bf16[8,32,1408]{2,1,0:T(8,128)(2,1)S(1)}, u32[]{:S(2)}, u32[]{:S(2)}) collective-permute-start(bf16[8,32,1408]{2,1,0:T(8,128)(2,1)S(1)} %get-tuple-element.22), channel_id=1, source_target_pairs={{0,8},{4,12},{8,16},{12,20},{16,24},{20,28},{24,0},{28,4},{32,40},... | collective-permute-start | bytes 2162696 | tf_op jit(solution)/shard_map/ppermute | solution.py:180
  65.8 18.9 %collective-permute-start.26 = (bf16[8,32,1408]{2,1,0:T(8,128)(2,1)S(1)}, bf16[8,32,1408]{2,1,0:T(8,128)(2,1)S(1)}, u32[]{:S(2)}, u32[]{:S(2)}) collective-permute-start(bf16[8,32,1408]{2,1,0:T(8,128)(2,1)S(1)} %get-tuple-element.24), channel_id=1, source_target_pairs={{0,24},{4,28},{8,0},{12,4},{16,8},{20,12},{24,16},{28,20},{32,56},... | collective-permute-start | bytes 2162696 | tf_op jit(solution)/shard_map/ppermute | solution.py:180
  68.8 17.0 %copy-start.2 = (bf16[4,32,1408]{2,1,0:T(8,128)(2,1)}, bf16[4,32,1408]{2,1,0:T(8,128)(2,1)S(1)}, u32[]{:S(2)}) copy-start(bf16[4,32,1408]{2,1,0:T(8,128)(2,1)S(1)} %collective-permute-done.3.refs_1_) | copy-start | bytes 1081348
  68.8 9.2 %collective-permute-start.4 = (bf16[4,32,1408]{2,1,0:T(8,128)(2,1)S(1)}, bf16[4,32,1408]{2,1,0:T(8,128)(2,1)S(1)}, u32[]{:S(2)}, u32[]{:S(2)}) collective-permute-start(bf16[4,32,1408]{2,1,0:T(8,128)(2,1)S(1)} %collective-permute-done.3.refs_1_), channel_id=1, source_target_pairs={{0,224},{4,228},{8,232},{12,236},{16,240},{20,244},{24,248},{28,25... | collective-permute-start | bytes 1081352 | tf_op jit(solution)/shard_map/ppermute | solution.py:180
  72.0 14.8 %copy-start.4 = (bf16[4,32,1408]{2,1,0:T(8,128)(2,1)}, bf16[4,32,1408]{2,1,0:T(8,128)(2,1)S(1)}, u32[]{:S(2)}) copy-start(bf16[4,32,1408]{2,1,0:T(8,128)(2,1)S(1)} %collective-permute-done.10.refs_8_) | copy-start | bytes 1081348
  72.0 6.0 %collective-permute-start.11 = (bf16[4,32,1408]{2,1,0:T(8,128)(2,1)S(1)}, bf16[4,32,1408]{2,1,0:T(8,128)(2,1)S(1)}, u32[]{:S(2)}, u32[]{:S(2)}) collective-permute-start(bf16[4,32,1408]{2,1,0:T(8,128)(2,1)S(1)} %collective-permute-done.3.refs_1_), channel_id=1, source_target_pairs={{0,4},{4,0},{8,12},{12,8},{16,20},{20,16},{24,28},{28,24},{32,36},... | collective-permute-start | bytes 1081352 | tf_op jit(solution)/shard_map/ppermute | solution.py:180
  74.3 15.8 %copy-start.6 = (bf16[4,32,1408]{2,1,0:T(8,128)(2,1)}, bf16[4,32,1408]{2,1,0:T(8,128)(2,1)S(1)}, u32[]{:S(2)}) copy-start(bf16[4,32,1408]{2,1,0:T(8,128)(2,1)S(1)} %collective-permute-done.7.refs_6_) | copy-start | bytes 1081348
  74.3 9.9 %collective-permute-start.8 = (bf16[4,32,1408]{2,1,0:T(8,128)(2,1)S(1)}, bf16[4,32,1408]{2,1,0:T(8,128)(2,1)}, u32[]{:S(2)}, u32[]{:S(2)}) collective-permute-start(bf16[4,32,1408]{2,1,0:T(8,128)(2,1)S(1)} %collective-permute-done.7.refs_6_), channel_id=1, source_target_pairs={{0,32},{4,36},{8,40},{12,44},{16,48},{20,52},{24,56},{28,60},{32,6... | collective-permute-start | bytes 1081352 | tf_op jit(solution)/shard_map/ppermute | solution.py:180
  78.0 19.4 %copy-start.8 = (bf16[4,32,1408]{2,1,0:T(8,128)(2,1)}, bf16[4,32,1408]{2,1,0:T(8,128)(2,1)S(1)}, u32[]{:S(2)}) copy-start(bf16[4,32,1408]{2,1,0:T(8,128)(2,1)S(1)} %collective-permute-done.4.refs_2_) | copy-start | bytes 1081348
  78.0 7.8 %collective-permute-start.17 = (bf16[4,32,1408]{2,1,0:T(8,128)(2,1)S(1)}, bf16[4,32,1408]{2,1,0:T(8,128)(2,1)S(1)}, u32[]{:S(2)}, u32[]{:S(2)}) collective-permute-start(bf16[4,32,1408]{2,1,0:T(8,128)(2,1)S(1)} %collective-permute-done.6.refs_7_), channel_id=1, source_target_pairs={{0,4},{4,0},{8,12},{12,8},{16,20},{20,16},{24,28},{28,24},{32,36},... | collective-permute-start | bytes 1081352 | tf_op jit(solution)/shard_map/ppermute | solution.py:180
  78.0 20.2 %copy-start.10 = (bf16[4,32,1408]{2,1,0:T(8,128)(2,1)}, bf16[4,32,1408]{2,1,0:T(8,128)(2,1)S(1)}, u32[]{:S(2)}) copy-start(bf16[4,32,1408]{2,1,0:T(8,128)(2,1)S(1)} %collective-permute-done.11.refs_9_) | copy-start | bytes 1081348
  78.0 12.0 %collective-permute-start.5 = (bf16[4,32,1408]{2,1,0:T(8,128)(2,1)S(1)}, bf16[4,32,1408]{2,1,0:T(8,128)(2,1)}, u32[]{:S(2)}, u32[]{:S(2)}) collective-permute-start(bf16[4,32,1408]{2,1,0:T(8,128)(2,1)S(1)} %collective-permute-done.4.refs_2_), channel_id=1, source_target_pairs={{0,224},{4,228},{8,232},{12,236},{16,240},{20,244},{24,248},{28,25... | collective-permute-start | bytes 1081352 | tf_op jit(solution)/shard_map/ppermute | solution.py:180
  84.2 12.5 %collective-permute-start.12 = (bf16[4,32,1408]{2,1,0:T(8,128)(2,1)S(1)}, bf16[4,32,1408]{2,1,0:T(8,128)(2,1)S(1)}, u32[]{:S(2)}, u32[]{:S(2)}) collective-permute-start(bf16[4,32,1408]{2,1,0:T(8,128)(2,1)S(1)} %collective-permute-done.4.refs_2_), channel_id=1, source_target_pairs={{0,4},{4,0},{8,12},{12,8},{16,20},{20,16},{24,28},{28,24},{32,36},... | collective-permute-start | bytes 1081352 | tf_op jit(solution)/shard_map/ppermute | solution.py:180
  84.2 17.3 %copy-start.23 = (bf16[8,32,1408]{2,1,0:T(8,128)(2,1)}, bf16[8,32,1408]{2,1,0:T(8,128)(2,1)S(1)}, u32[]{:S(2)}) copy-start(bf16[8,32,1408]{2,1,0:T(8,128)(2,1)S(1)} %collective-permute-done.27) | copy-start | bytes 2162692
  84.2 13.2 %collective-permute-start.16 = (bf16[4,32,1408]{2,1,0:T(8,128)(2,1)S(1)}, bf16[4,32,1408]{2,1,0:T(8,128)(2,1)S(1)}, u32[]{:S(2)}, u32[]{:S(2)}) collective-permute-start(bf16[4,32,1408]{2,1,0:T(8,128)(2,1)S(1)} %collective-permute-done.7.refs_6_), channel_id=1, source_target_pairs={{0,4},{4,0},{8,12},{12,8},{16,20},{20,16},{24,28},{28,24},{32,36},... | collective-permute-start | bytes 1081352 | tf_op jit(solution)/shard_map/ppermute | solution.py:180
  84.7 16.7 %copy-start.25 = (bf16[8,32,1408]{2,1,0:T(8,128)(2,1)}, bf16[8,32,1408]{2,1,0:T(8,128)(2,1)S(1)}, u32[]{:S(2)}) copy-start(bf16[8,32,1408]{2,1,0:T(8,128)(2,1)S(1)} %collective-permute-done.26) | copy-start | bytes 2162692
  84.7 11.9 %collective-permute-start.9 = (bf16[4,32,1408]{2,1,0:T(8,128)(2,1)}, bf16[4,32,1408]{2,1,0:T(8,128)(2,1)}, u32[]{:S(2)}, u32[]{:S(2)}) collective-permute-start(bf16[4,32,1408]{2,1,0:T(8,128)(2,1)} %collective-permute-done.8.refs_5_), channel_id=1, source_target_pairs={{0,32},{4,36},{8,40},{12,44},{16,48},{20,52},{24,56},{28,60},{32,6... | collective-permute-start | bytes 1081352 | tf_op jit(solution)/shard_map/ppermute | solution.py:180
  86.6 17.2 %collective-permute-start.15 = (bf16[4,32,1408]{2,1,0:T(8,128)(2,1)}, bf16[4,32,1408]{2,1,0:T(8,128)(2,1)}, u32[]{:S(2)}, u32[]{:S(2)}) collective-permute-start(bf16[4,32,1408]{2,1,0:T(8,128)(2,1)} %collective-permute-done.8.refs_5_), channel_id=1, source_target_pairs={{0,4},{4,0},{8,12},{12,8},{16,20},{20,16},{24,28},{28,24},{32,36},... | collective-permute-start | bytes 1081352 | tf_op jit(solution)/shard_map/ppermute | solution.py:180
  90.1 13.7 %collective-permute-start.13 = (bf16[4,32,1408]{2,1,0:T(8,128)(2,1)}, bf16[4,32,1408]{2,1,0:T(8,128)(2,1)}, u32[]{:S(2)}, u32[]{:S(2)}) collective-permute-start(bf16[4,32,1408]{2,1,0:T(8,128)(2,1)} %collective-permute-done.5.refs_3_), channel_id=1, source_target_pairs={{0,4},{4,0},{8,12},{12,8},{16,20},{20,16},{24,28},{28,24},{32,36},... | collective-permute-start | bytes 1081352 | tf_op jit(solution)/shard_map/ppermute | solution.py:180
  96.7 7.1 %collective-permute-start.14 = (bf16[4,32,1408]{2,1,0:T(8,128)(2,1)}, bf16[4,32,1408]{2,1,0:T(8,128)(2,1)}, u32[]{:S(2)}, u32[]{:S(2)}) collective-permute-start(bf16[4,32,1408]{2,1,0:T(8,128)(2,1)} %collective-permute-done.9.refs_4_), channel_id=1, source_target_pairs={{0,4},{4,0},{8,12},{12,8},{16,20},{20,16},{24,28},{28,24},{32,36},... | collective-permute-start | bytes 1081352 | tf_op jit(solution)/shard_map/ppermute | solution.py:180
  97.4 33.0 %collective-permute-start.28 = (bf16[4,32,1408]{2,1,0:T(8,128)(2,1)}, bf16[4,32,1408]{2,1,0:T(8,128)(2,1)}, u32[]{:S(2)}, u32[]{:S(2)}) collective-permute-start(bf16[4,32,1408]{2,1,0:T(8,128)(2,1)} %get-tuple-element.30), channel_id=1, source_target_pairs={{0,8},{4,12},{8,16},{12,20},{16,24},{20,28},{24,0},{28,4},{32,40},... | collective-permute-start | bytes 1081352 | tf_op jit(solution)/shard_map/ppermute | solution.py:180
  98.2 32.2 %collective-permute-start.29 = (bf16[4,32,1408]{2,1,0:T(8,128)(2,1)}, bf16[4,32,1408]{2,1,0:T(8,128)(2,1)}, u32[]{:S(2)}, u32[]{:S(2)}) collective-permute-start(bf16[4,32,1408]{2,1,0:T(8,128)(2,1)} %get-tuple-element.31), channel_id=1, source_target_pairs={{0,24},{4,28},{8,0},{12,4},{16,8},{20,12},{24,16},{28,20},{32,56},... | collective-permute-start | bytes 1081352 | tf_op jit(solution)/shard_map/ppermute | solution.py:180
  103.8 1.5 copy-start
  105.3 1.0 copy-start.3
  106.3 1.0 copy-start.5
  107.3 1.0 copy-start.7
  108.2 1.0 copy-start.9
  109.2 1.0 copy-start.11
  110.2 1.0 copy-start.13
  111.2 1.0 copy-start.15
  112.2 1.0 copy-start.17
  113.2 17.2 %copy-start.18 = (f32[1,8,32,1408]{3,2,1,0:T(8,128)S(1)}, f32[1,8,32,1408]{3,2,1,0:T(8,128)}, u32[]{:S(2)}) copy-start(f32[1,8,32,1408]{3,2,1,0:T(8,128)} %get-tuple-element.25) | copy-start | bytes 4325380
  113.2 17.2 %copy-start.24 = (bf16[8,32,1408]{2,1,0:T(8,128)(2,1)S(1)}, bf16[8,32,1408]{2,1,0:T(8,128)(2,1)}, u32[]{:S(2)}) copy-start(bf16[8,32,1408]{2,1,0:T(8,128)(2,1)} %copy-done.23) | copy-start | bytes 2162692
  113.2 17.3 %copy-start.26 = (bf16[8,32,1408]{2,1,0:T(8,128)(2,1)S(1)}, bf16[8,32,1408]{2,1,0:T(8,128)(2,1)}, u32[]{:S(2)}) copy-start(bf16[8,32,1408]{2,1,0:T(8,128)(2,1)} %copy-done.25) | copy-start | bytes 2162692
  127.1 31.9 %collective-permute-start.20 = (bf16[160,2048]{1,0:T(8,128)(2,1)S(1)}, bf16[160,2048]{1,0:T(8,128)(2,1)S(1)}, u32[]{:S(2)}, u32[]{:S(2)}) collective-permute-start(bf16[160,2048]{1,0:T(8,128)(2,1)S(1)} %get-tuple-element.16), channel_id=1, source_target_pairs={{0,3},{1,0},{2,1},{3,2},{4,7},{5,4},{6,5},{7,6},{8,11},{9,8},{10,9... | collective-permute-start | bytes 1966088 | tf_op jit(solution)/shard_map/ppermute | solution.py:184
  127.2 32.8 %collective-permute-start.19 = (bf16[160,2048]{1,0:T(8,128)(2,1)S(1)}, bf16[160,2048]{1,0:T(8,128)(2,1)S(1)}, u32[]{:S(2)}, u32[]{:S(2)}) collective-permute-start(bf16[160,2048]{1,0:T(8,128)(2,1)S(1)} %get-tuple-element.15), channel_id=1, source_target_pairs={{0,1},{1,2},{2,3},{3,0},{4,5},{5,6},{6,7},{7,4},{8,9},{9,10},{10,1... | collective-permute-start | bytes 1966088 | tf_op jit(solution)/shard_map/ppermute | solution.py:184
  130.4 31.5 %collective-permute-start.18 = (bf16[160,2048]{1,0:T(8,128)(2,1)S(1)}, bf16[160,2048]{1,0:T(8,128)(2,1)S(1)}, u32[]{:S(2)}, u32[]{:S(2)}) collective-permute-start(bf16[160,2048]{1,0:T(8,128)(2,1)S(1)} %get-tuple-element.14), channel_id=1, source_target_pairs={{0,2},{1,3},{2,0},{3,1},{4,6},{5,7},{6,4},{7,5},{8,10},{9,11},{10,... | collective-permute-start | bytes 1966088 | tf_op jit(solution)/shard_map/ppermute | solution.py:184
  130.4 4.1 %copy-start.21 = (bf16[640,1408]{1,0:T(8,128)(2,1)S(1)}, bf16[640,1408]{1,0:T(8,128)(2,1)}, u32[]{:S(2)}) copy-start(bf16[640,1408]{1,0:T(8,128)(2,1)} %param.9) | copy-start | bytes 5406724
  130.4 4.1 %copy-start.22 = (bf16[640,1408]{1,0:T(8,128)(2,1)S(1)}, bf16[640,1408]{1,0:T(8,128)(2,1)}, u32[]{:S(2)}) copy-start(bf16[640,1408]{1,0:T(8,128)(2,1)} %param.10) | copy-start | bytes 5406724
  132.1 32.3 %collective-permute-start.36 = (bf16[32,1408]{1,0:T(8,128)(2,1)S(1)}, bf16[32,1408]{1,0:T(8,128)(2,1)S(1)}, u32[]{:S(2)}, u32[]{:S(2)}) collective-permute-start(bf16[32,1408]{1,0:T(8,128)(2,1)S(1)} %fusion.52), channel_id=1, source_target_pairs={{0,224},{4,228},{8,232},{12,236},{16,240},{20,244},{24,248},{28,25... | collective-permute-start | bytes 270344 | tf_op jit(solution)/shard_map/ppermute | solution.py:180
  133.7 32.1 %collective-permute-start.35 = (bf16[32,1408]{1,0:T(8,128)(2,1)S(1)}, bf16[32,1408]{1,0:T(8,128)(2,1)S(1)}, u32[]{:S(2)}, u32[]{:S(2)}) collective-permute-start(bf16[32,1408]{1,0:T(8,128)(2,1)S(1)} %get-tuple-element.37), channel_id=1, source_target_pairs={{0,32},{4,36},{8,40},{12,44},{16,48},{20,52},{24,56},{28,60},{32,6... | collective-permute-start | bytes 270344 | tf_op jit(solution)/shard_map/ppermute | solution.py:180
  140.9 37.8 %copy-start.28 = (f32[1408,32]{0,1:T(8,128)S(1)}, f32[1408,32]{0,1:T(8,128)}, u32[]{:S(2)}) copy-start(f32[1408,32]{0,1:T(8,128)} %param.13) | copy-start | bytes 540676
  159.0 12.4 %collective-permute-start.34 = (bf16[32,1408]{1,0:T(8,128)(2,1)S(1)}, bf16[32,1408]{1,0:T(8,128)(2,1)S(1)}, u32[]{:S(2)}, u32[]{:S(2)}) collective-permute-start(bf16[32,1408]{1,0:T(8,128)(2,1)S(1)} %get-tuple-element.36), channel_id=1, source_target_pairs={{0,192},{4,196},{8,200},{12,204},{16,208},{20,212},{24,216},{28,22... | collective-permute-start | bytes 270344 | tf_op jit(solution)/shard_map/ppermute | solution.py:180
  159.9 11.5 %collective-permute-start.33 = (bf16[32,1408]{1,0:T(8,128)(2,1)S(1)}, bf16[32,1408]{1,0:T(8,128)(2,1)S(1)}, u32[]{:S(2)}, u32[]{:S(2)}) collective-permute-start(bf16[32,1408]{1,0:T(8,128)(2,1)S(1)} %get-tuple-element.35), channel_id=1, source_target_pairs={{0,64},{4,68},{8,72},{12,76},{16,80},{20,84},{24,88},{28,92},{32,9... | collective-permute-start | bytes 270344 | tf_op jit(solution)/shard_map/ppermute | solution.py:180
  161.9 9.5 %collective-permute-start.32 = (bf16[32,1408]{1,0:T(8,128)(2,1)S(1)}, bf16[32,1408]{1,0:T(8,128)(2,1)S(1)}, u32[]{:S(2)}, u32[]{:S(2)}) collective-permute-start(bf16[32,1408]{1,0:T(8,128)(2,1)S(1)} %get-tuple-element.34), channel_id=1, source_target_pairs={{0,160},{4,164},{8,168},{12,172},{16,176},{20,180},{24,184},{28,18... | collective-permute-start | bytes 270344 | tf_op jit(solution)/shard_map/ppermute | solution.py:180
  164.3 11.4 %collective-permute-start.31 = (bf16[32,1408]{1,0:T(8,128)(2,1)S(1)}, bf16[32,1408]{1,0:T(8,128)(2,1)S(1)}, u32[]{:S(2)}, u32[]{:S(2)}) collective-permute-start(bf16[32,1408]{1,0:T(8,128)(2,1)S(1)} %get-tuple-element.33), channel_id=1, source_target_pairs={{0,96},{4,100},{8,104},{12,108},{16,112},{20,116},{24,120},{28,124... | collective-permute-start | bytes 270344 | tf_op jit(solution)/shard_map/ppermute | solution.py:180
  165.8 12.9 %collective-permute-start.30 = (bf16[32,1408]{1,0:T(8,128)(2,1)S(1)}, bf16[32,1408]{1,0:T(8,128)(2,1)S(1)}, u32[]{:S(2)}, u32[]{:S(2)}) collective-permute-start(bf16[32,1408]{1,0:T(8,128)(2,1)S(1)} %get-tuple-element.32), channel_id=1, source_target_pairs={{0,128},{4,132},{8,136},{12,140},{16,144},{20,148},{24,152},{28,15... | collective-permute-start | bytes 270344 | tf_op jit(solution)/shard_map/ppermute | solution.py:180
  (3 other events, 2.3 us)

commit v3 on v2

--- a/solution.py
+++ b/solution.py
@@ -80,10 +80,9 @@
         for zr, block in enumerate(blocks):
             yr = 0
             for piece in block:
-                for j in range(piece.shape[0]):
-                    places.append((zr, cr, yr, len(pieces), j))
-                    yr += 1
+                places.append((zr, cr, yr))
                 pieces.append(piece)
+                yr += piece.shape[0]
     n = len(pieces)
 
     def body(where, hidden, *refs):
@@ -93,31 +92,28 @@
         step = pl.program_id(0)
         y, c, t = where[1], where[2], where[3]
 
-        def copies(at):
-            return [
-                pltpu.make_async_copy(
-                    blocks[i].at[j],
-                    weight.at[zr, lax.rem(y + yr, NY), lax.rem(c + cr, NC)],
-                    sems.at[zr, cr, yr],
-                )
-                for zr, cr, yr, i, j in places
-                if zr == at
-            ]
-
         @pl.when(step == 0)
         def _():
-            for zr in range(count):
-                for copy in copies(zr):
-                    copy.start()
+            for block, (zr, cr, first) in zip(blocks, places):
+
+                def send(j, _, block=block, zr=zr, cr=cr, first=first):
+                    yr = first + j
+                    pltpu.make_async_copy(
+                        block.at[j],
+                        weight.at[zr, lax.rem(y + yr, NY), lax.rem(c + cr, NC)],
+                        sems.at[zr, cr, yr],
+                    ).start()
+                    return 0
+
+                lax.fori_loop(0, block.shape[0], send, 0)
             for i in range(parts):
                 ordered[pl.ds(i * rows, rows), :] = hidden[lax.rem(t + i, parts)]
 
-        for zr in range(count):
-
-            @pl.when(step == zr)
-            def _(zr=zr):
-                for copy in copies(zr):
-                    copy.wait()
+        for cr in range(NC):
+            for yr in range(NY):
+                pltpu.make_async_copy(
+                    blocks[0].at[0], weight.at[step, yr, cr], sems.at[step, cr, yr]
+                ).wait()
 
         part = lax.dot_general(
             ordered[...],
@@ -239,8 +235,9 @@
     up = shift(up_y.astype(BF), dy=1)
     dn = shift(dn_y.astype(BF), dy=-1)
 
-    far = shift(up3, dz=1)
+    far_u, far_d = shift(up3[:2], dz=1), shift(dn3[2:], dz=-1)
     c3, c5 = shift(dn3, dc=1), shift(up3, dc=1)
+    far = jnp.concatenate([far_u, far_d])
     c4 = shift(far, dc=1)
     own = [[wy], [dn1], [dn2], [dn3], [far], [up3], [up2], [up1]]
     other = [[c0], [c1], [c2], [c3], [c4], [c5], [c6], [c7]]

time: 180 us -> 185 us (1.028)
  the two profiles are of different devices: /device:TPU:6 before, /device:TPU:2 now
where the time goes in v3:
time: 185 us; the launch traced here: 181 us
  waiting for transfers between devices  69.2 us (37%)
  starting transfers between devices  50.4 us (27%)
  Pallas kernels  20.5 us (11%)
  local copies, waits for them, and re-layouts  20.2 us (11%)
  other arithmetic  13.6 us (7%)
  matrix products  6.41 us (3%)
    ppermute x31, waiting for transfers between devices, shift(): return lax.ppermute(x, 'fs', perm)  40.1 us
    ppermute x31, starting transfers between devices, shift(): return lax.ppermute(x, 'fs', perm)  36.8 us
    ppermute x7, waiting for transfers between devices, shift_x(): return lax.ppermute(x, 'tp', [(i, (i + d) % NX) for i in range(NX)])  29.1 us
    unnamed x63, local copies, waits for them, and re-layouts  14.8 us
    ppermute x7, starting transfers between devices, shift_x(): return lax.ppermute(x, 'tp', [(i, (i + d) % NX) for i in range(NX)])  13.5 us
    pallas_call x1, Pallas kernels, partial_products(): pl.pallas_call(body, grid_spec=pltpu.PrefetchScalarGridSpec(num_scalar_pr...  13.5 us
    pallas_call x1, Pallas kernels, grad_term(): pl.pallas_call(body, grid_spec=pltpu.PrefetchScalarGridSpec(num_scalar_pr...  7 us
    dot_general x1, matrix products, step(): jnp.dot(cot_rows, whole.reshape(d, ff), preferred_element_type=F32)  6.41 us
  transfers between devices with their start and end apart: 38, of which 14 were waited for; matrix products, arithmetic and copies ran while one was open for 14% of the time, Pallas kernels for 7%

profile of v3, /device:TPU:2, one launch (start us, length us, event | category | flops | bytes accessed | tf_op | source)
XLA Modules:
  0.0 181.2 jit_solution(9548354513364292074)
XLA Ops:
  0.6 2.3 %collective-permute-start.22 = (bf16[160,2048]{1,0:T(8,128)(2,1)}, bf16[160,2048]{1,0:T(8,128)(2,1)S(1)}, u32[]{:S(2)}, u32[]{:S(2)}) collective-permute-start(bf16[160,2048]{1,0:T(8,128)(2,1)} %param.11), channel_id=1, source_target_pairs={{0,3},{1,0},{2,1},{3,2},{4,7},{5,4},{6,5},{7,6},{8,11},{9,8},{10,9... | collective-permute-start | bytes 1966088 | tf_op jit(solution)/shard_map/ppermute | solution.py:180
  3.0 4.3 %fusion.16.hidden = bf16[640,1408]{1,0:T(8,128)(2,1)} fusion(bf16[640,1408]{1,0:T(8,128)(2,1)} %param.10, bf16[640,1408]{1,0:T(8,128)(2,1)} %param.9), kind=kLoop, calls=%fused_computation.23 | loop fusion | flops 7208960 | bytes 5406720 | tf_op jit(solution)/shard_map/convert_element_type | solution.py:216
  7.7 1.1 bitcast_dynamic-update-slice_fusion.2
  8.9 9.9 %collective-permute-done.23 = bf16[160,2048]{1,0:T(8,128)(2,1)} collective-permute-done((bf16[160,2048]{1,0:T(8,128)(2,1)}, bf16[160,2048]{1,0:T(8,128)(2,1)}, u32[]{:S(2)}, u32[]{:S(2)}) %collective-permute-start.23) | collective-permute-done | bytes 655392 | tf_op jit(solution)/shard_map/ppermute | solution.py:180
  18.8 1.0 slice.98
  19.8 0.5 collective-permute-start.24
  20.3 2.6 %collective-permute-start.25 = (bf16[80,2048]{1,0:T(8,128)(2,1)S(1)}, bf16[80,2048]{1,0:T(8,128)(2,1)S(1)}, u32[]{:S(2)}, u32[]{:S(2)}) collective-permute-start(bf16[80,2048]{1,0:T(8,128)(2,1)S(1)} %slice.99), channel_id=1, source_target_pairs={{0,3},{1,0},{2,1},{3,2},{4,7},{5,4},{6,5},{7,6},{8,11},{9,8},{10,9... | collective-permute-start | bytes 983048 | tf_op jit(solution)/shard_map/ppermute | solution.py:180
  23.0 1.1 bitcast_dynamic-update-slice_fusion
  24.1 5.2 %collective-permute-done.24 = bf16[80,2048]{1,0:T(8,128)(2,1)S(1)} collective-permute-done((bf16[80,2048]{1,0:T(8,128)(2,1)S(1)}, bf16[80,2048]{1,0:T(8,128)(2,1)S(1)}, u32[]{:S(2)}, u32[]{:S(2)}) %collective-permute-start.24) | collective-permute-done | bytes 327712 | tf_op jit(solution)/shard_map/ppermute | solution.py:180
  29.5 7.0 %grad_term.1 = (bf16[4,8,32,1408]{3,2,1,0:T(8,128)(2,1)S(1)}, bf16[4,8,32,1408]{3,2,1,0:T(8,128)(2,1)S(1)}) custom-call(s32[4]{0:T(128)S(1)} %pad_add_fusion.where, bf16[640,2048]{1,0:T(8,128)(2,1)S(1)} %bitcast.78, bf16[640,1408]{1,0:T(8,128)(2,1)S(1)} %copy-done.1), custom_call_target="tpu_custom_call" | custom-call | flops 3690987520 | bytes 12582912 | tf_op jit(solution)/shard_map/grad_term/pallas_call | solution.py:44
  36.6 1.6 collective-permute-start.2
  38.2 2.9 %collective-permute-start.1 = (bf16[32,1408]{1,0:T(8,128)(2,1)S(1)}, bf16[32,1408]{1,0:T(8,128)(2,1)S(1)}, u32[]{:S(2)}, u32[]{:S(2)}) collective-permute-start(bf16[32,1408]{1,0:T(8,128)(2,1)S(1)} %bitcast.83), channel_id=1, source_target_pairs={{0,16},{4,20},{8,24},{12,28},{16,0},{20,4},{24,8},{28,12},{32,48},... | collective-permute-start | bytes 270344 | tf_op jit(solution)/shard_map/ppermute | solution.py:176
  41.2 1.3 collective-permute-start
  42.9 3.1 %collective-permute-done.1 = bf16[32,1408]{1,0:T(8,128)(2,1)S(1)} collective-permute-done((bf16[32,1408]{1,0:T(8,128)(2,1)S(1)}, bf16[32,1408]{1,0:T(8,128)(2,1)S(1)}, u32[]{:S(2)}, u32[]{:S(2)}) %collective-permute-start.1) | collective-permute-done | bytes 90144 | tf_op jit(solution)/shard_map/ppermute | solution.py:176
  46.1 5.9 %collective-permute-start.3 = (bf16[4,32,1408]{2,1,0:T(8,128)(2,1)S(1)}, bf16[4,32,1408]{2,1,0:T(8,128)(2,1)S(1)}, u32[]{:S(2)}, u32[]{:S(2)}) collective-permute-start(bf16[4,32,1408]{2,1,0:T(8,128)(2,1)S(1)} %pad_maximum_fusion.refs_0_), channel_id=1, source_target_pairs={{0,224},{4,228},{8,232},{12,236},{16,240},{20,244},{24,248},{28,25... | collective-permute-start | bytes 1081352 | tf_op jit(solution)/shard_map/ppermute | solution.py:176
  52.0 7.4 %collective-permute-done.3.refs_1_ = bf16[4,32,1408]{2,1,0:T(8,128)(2,1)S(1)} collective-permute-done((bf16[4,32,1408]{2,1,0:T(8,128)(2,1)S(1)}, bf16[4,32,1408]{2,1,0:T(8,128)(2,1)S(1)}, u32[]{:S(2)}, u32[]{:S(2)}) %collective-permute-start.3) | collective-permute-done | bytes 360480 | tf_op jit(solution)/shard_map/ppermute | solution.py:176
  59.4 3.7 %collective-permute-start.4 = (bf16[4,32,1408]{2,1,0:T(8,128)(2,1)S(1)}, bf16[4,32,1408]{2,1,0:T(8,128)(2,1)S(1)}, u32[]{:S(2)}, u32[]{:S(2)}) collective-permute-start(bf16[4,32,1408]{2,1,0:T(8,128)(2,1)S(1)} %collective-permute-done.3.refs_1_), channel_id=1, source_target_pairs={{0,224},{4,228},{8,232},{12,236},{16,240},{20,244},{24,248},{28,25... | collective-permute-start | bytes 1081352 | tf_op jit(solution)/shard_map/ppermute | solution.py:176
  63.1 6.5 %collective-permute-done.4.refs_2_ = bf16[4,32,1408]{2,1,0:T(8,128)(2,1)S(1)} collective-permute-done((bf16[4,32,1408]{2,1,0:T(8,128)(2,1)S(1)}, bf16[4,32,1408]{2,1,0:T(8,128)(2,1)S(1)}, u32[]{:S(2)}, u32[]{:S(2)}) %collective-permute-start.4) | collective-permute-done | bytes 360480 | tf_op jit(solution)/shard_map/ppermute | solution.py:176
  69.6 3.7 %collective-permute-start.5 = (bf16[4,32,1408]{2,1,0:T(8,128)(2,1)S(1)}, bf16[4,32,1408]{2,1,0:T(8,128)(2,1)S(1)}, u32[]{:S(2)}, u32[]{:S(2)}) collective-permute-start(bf16[4,32,1408]{2,1,0:T(8,128)(2,1)S(1)} %collective-permute-done.4.refs_2_), channel_id=1, source_target_pairs={{0,224},{4,228},{8,232},{12,236},{16,240},{20,244},{24,248},{28,25... | collective-permute-start | bytes 1081352 | tf_op jit(solution)/shard_map/ppermute | solution.py:176
  73.3 1.8 fusion.19
  75.1 3.2 %collective-permute-start.27 = (bf16[8,32,1408]{2,1,0:T(8,128)(2,1)S(1)}, bf16[8,32,1408]{2,1,0:T(8,128)(2,1)S(1)}, u32[]{:S(2)}, u32[]{:S(2)}) collective-permute-start(bf16[8,32,1408]{2,1,0:T(8,128)(2,1)S(1)} %get-tuple-element.24), channel_id=1, source_target_pairs={{0,24},{4,28},{8,0},{12,4},{16,8},{20,12},{24,16},{28,20},{32,56},... | collective-permute-start | bytes 2162696 | tf_op jit(solution)/shard_map/ppermute | solution.py:176
  78.4 4.1 %collective-permute-done.8.refs_5_ = bf16[4,32,1408]{2,1,0:T(8,128)(2,1)} collective-permute-done((bf16[4,32,1408]{2,1,0:T(8,128)(2,1)S(1)}, bf16[4,32,1408]{2,1,0:T(8,128)(2,1)}, u32[]{:S(2)}, u32[]{:S(2)}) %collective-permute-start.8) | collective-permute-done | bytes 360480 | tf_op jit(solution)/shard_map/ppermute | solution.py:176
  82.5 0.9 slice.96
  83.7 0.5 collective-permute-start.12
  84.2 6.1 %collective-permute-done.9 = bf16[2,32,1408]{2,1,0:T(8,128)(2,1)S(1)} collective-permute-done((bf16[2,32,1408]{2,1,0:T(8,128)(2,1)S(1)}, bf16[2,32,1408]{2,1,0:T(8,128)(2,1)S(1)}, u32[]{:S(2)}, u32[]{:S(2)}) %collective-permute-start.9) | collective-permute-done | bytes 180256 | tf_op jit(solution)/shard_map/ppermute | solution.py:176
  90.2 0.7 constant_dynamic-update-slice_fusion.1
  90.9 4.8 %collective-permute-done.10 = bf16[2,32,1408]{2,1,0:T(8,128)(2,1)S(1)} collective-permute-done((bf16[2,32,1408]{2,1,0:T(8,128)(2,1)S(1)}, bf16[2,32,1408]{2,1,0:T(8,128)(2,1)S(1)}, u32[]{:S(2)}, u32[]{:S(2)}) %collective-permute-start.10) | collective-permute-done | bytes 180256 | tf_op jit(solution)/shard_map/ppermute | solution.py:176
  95.7 0.7 constant_dynamic-update-slice_fusion.refs_4_
  96.4 0.6 collective-permute-start.13
  97.2 1.0 fusion.26
  98.2 0.7 copy-done.10
  98.9 0.5 collective-permute-start.14
  99.4 0.8 copy-done.12
  100.2 0.7 copy-done.14
  101.4 0.7 copy-done.16
  102.2 0.8 copy-done.18
  102.9 3.2 %collective-permute-start.30 = (bf16[4,32,1408]{2,1,0:T(8,128)(2,1)}, bf16[4,32,1408]{2,1,0:T(8,128)(2,1)}, u32[]{:S(2)}, u32[]{:S(2)}) collective-permute-start(bf16[4,32,1408]{2,1,0:T(8,128)(2,1)} %get-tuple-element.31), channel_id=1, source_target_pairs={{0,24},{4,28},{8,0},{12,4},{16,8},{20,12},{24,16},{28,20},{32,56},... | collective-permute-start | bytes 1081352 | tf_op jit(solution)/shard_map/ppermute | solution.py:176
  106.2 2.3 %fusion.17 = bf16[640,1408]{1,0:T(8,128)(2,1)} fusion(bf16[640,1408]{1,0:T(8,128)(2,1)S(1)} %copy-done.21, bf16[640,1408]{1,0:T(8,128)(2,1)S(1)} %copy-done.22), kind=kLoop, calls=%fused_computation.24 | loop fusion | flops 7208960 | bytes 5406720 | tf_op jit(solution)/shard_map/convert_element_type | solution.py:211
  108.5 1.5 copy-done
  110.0 1.0 copy-done.3
  111.0 1.0 copy-done.5
  112.0 1.0 copy-done.7
  112.9 1.0 copy-done.9
  113.9 1.0 copy-done.11
  114.9 1.0 copy-done.13
  115.9 1.0 copy-done.15
  116.9 1.0 copy-done.17
  117.9 1.0 copy-done.19
  118.9 13.5 %partial_products.1 = (bf16[160,2048]{1,0:T(8,128)(2,1)S(1)}, bf16[160,2048]{1,0:T(8,128)(2,1)S(1)}, bf16[160,2048]{1,0:T(8,128)(2,1)S(1)}, bf16[160,2048]{1,0:T...) custom-call(s32[4]{0:T(128)S(1)} %pad_add_fusion.where, bf16[4,160,1408]{2,1,0:T(8,128)(2,1)S(1)} %bitcast.80, ...), custom_call_target="tpu_custom_call" | custom-call | flops 3690987520 | bytes 16777216 | tf_op jit(solution)/shard_map/partial_products/pallas_call | solution.py:131
  132.4 3.0 %collective-permute-start.21 = (bf16[160,2048]{1,0:T(8,128)(2,1)S(1)}, bf16[160,2048]{1,0:T(8,128)(2,1)S(1)}, u32[]{:S(2)}, u32[]{:S(2)}) collective-permute-start(bf16[160,2048]{1,0:T(8,128)(2,1)S(1)} %get-tuple-element.16), channel_id=1, source_target_pairs={{0,3},{1,0},{2,1},{3,2},{4,7},{5,4},{6,5},{7,6},{8,11},{9,8},{10,9... | collective-permute-start | bytes 1966088 | tf_op jit(solution)/shard_map/ppermute | solution.py:180
  135.4 5.1 %collective-permute-start.19 = (bf16[160,2048]{1,0:T(8,128)(2,1)S(1)}, bf16[160,2048]{1,0:T(8,128)(2,1)S(1)}, u32[]{:S(2)}, u32[]{:S(2)}) collective-permute-start(bf16[160,2048]{1,0:T(8,128)(2,1)S(1)} %get-tuple-element.14), channel_id=1, source_target_pairs={{0,2},{1,3},{2,0},{3,1},{4,6},{5,7},{6,4},{7,5},{8,10},{9,11},{10,... | collective-permute-start | bytes 1966088 | tf_op jit(solution)/shard_map/ppermute | solution.py:180
  140.5 1.5 fusion.29
  142.1 1.3 collective-permute-start.37
  143.7 0.9 collective-permute-start.36
  144.6 6.4 %fusion.15 = (bf16[640,1408]{1,0:T(8,128)(2,1)}, bf16[640,1408]{1,0:T(8,128)(2,1)}) fusion(bf16[640,1408]{1,0:T(8,128)(2,1)S(1)} %copy-done.23, bf16[640,1408]{1,0:T(8,128)(2,1)S(1)} %copy-done.24, bf16[640,2048]{1,0:T(8,128)(2,1)S(1)} %bitcast.79, bf16[2048,1408]{1,0:T(8,128)(2,1)S(1)} %bitcast.81), kind=kOutput, calls=%fused_computation.22 | convolution fusion | flops 3704504320 | bytes 15597568 | tf_op jit(solution)/shard_map/dot_general | solution.py:264
  151.0 0.7 collective-permute-start.35
  151.7 2.3 %collective-permute-done.20 = bf16[160,2048]{1,0:T(8,128)(2,1)S(1)} collective-permute-done((bf16[160,2048]{1,0:T(8,128)(2,1)S(1)}, bf16[160,2048]{1,0:T(8,128)(2,1)S(1)}, u32[]{:S(2)}, u32[]{:S(2)}) %collective-permute-start.20) | collective-permute-done | bytes 655392 | tf_op jit(solution)/shard_map/ppermute | solution.py:180
  154.0 11.7 %collective-permute-done.19 = bf16[160,2048]{1,0:T(8,128)(2,1)S(1)} collective-permute-done((bf16[160,2048]{1,0:T(8,128)(2,1)S(1)}, bf16[160,2048]{1,0:T(8,128)(2,1)S(1)}, u32[]{:S(2)}, u32[]{:S(2)}) %collective-permute-start.19) | collective-permute-done | bytes 655392 | tf_op jit(solution)/shard_map/ppermute | solution.py:180
  165.7 3.8 %collective-permute-start.32 = (bf16[32,1408]{1,0:T(8,128)(2,1)S(1)}, bf16[32,1408]{1,0:T(8,128)(2,1)S(1)}, u32[]{:S(2)}, u32[]{:S(2)}) collective-permute-start(bf16[32,1408]{1,0:T(8,128)(2,1)S(1)} %get-tuple-element.33), channel_id=1, source_target_pairs={{0,96},{4,100},{8,104},{12,108},{16,112},{20,116},{24,120},{28,124... | collective-permute-start | bytes 270344 | tf_op jit(solution)/shard_map/ppermute | solution.py:176
  169.5 2.0 %collective-permute-start.31 = (bf16[32,1408]{1,0:T(8,128)(2,1)S(1)}, bf16[32,1408]{1,0:T(8,128)(2,1)S(1)}, u32[]{:S(2)}, u32[]{:S(2)}) collective-permute-start(bf16[32,1408]{1,0:T(8,128)(2,1)S(1)} %get-tuple-element.32), channel_id=1, source_target_pairs={{0,128},{4,132},{8,136},{12,140},{16,144},{20,148},{24,152},{28,15... | collective-permute-start | bytes 270344 | tf_op jit(solution)/shard_map/ppermute | solution.py:176
  171.5 1.3 add_convert_fusion.2
  173.2 3.6 %collective-permute-done.32 = bf16[32,1408]{1,0:T(8,128)(2,1)S(1)} collective-permute-done((bf16[32,1408]{1,0:T(8,128)(2,1)S(1)}, bf16[32,1408]{1,0:T(8,128)(2,1)S(1)}, u32[]{:S(2)}, u32[]{:S(2)}) %collective-permute-start.32) | collective-permute-done | bytes 90144 | tf_op jit(solution)/shard_map/ppermute | solution.py:176
  176.8 3.6 %collective-permute-done.31 = bf16[32,1408]{1,0:T(8,128)(2,1)S(1)} collective-permute-done((bf16[32,1408]{1,0:T(8,128)(2,1)S(1)}, bf16[32,1408]{1,0:T(8,128)(2,1)S(1)}, u32[]{:S(2)}, u32[]{:S(2)}) %collective-permute-start.31) | collective-permute-done | bytes 90144 | tf_op jit(solution)/shard_map/ppermute | solution.py:176
  180.4 0.8 fusion.37
  (100 shorter events, 2.9 us)
Async XLA Ops:
  0.6 19.7 %collective-permute-start.22 = (bf16[160,2048]{1,0:T(8,128)(2,1)}, bf16[160,2048]{1,0:T(8,128)(2,1)S(1)}, u32[]{:S(2)}, u32[]{:S(2)}) collective-permute-start(bf16[160,2048]{1,0:T(8,128)(2,1)} %param.11), channel_id=1, source_target_pairs={{0,3},{1,0},{2,1},{3,2},{4,7},{5,4},{6,5},{7,6},{8,11},{9,8},{10,9... | collective-permute-start | bytes 1966088 | tf_op jit(solution)/shard_map/ppermute | solution.py:180
  2.9 15.8 %collective-permute-start.23 = (bf16[160,2048]{1,0:T(8,128)(2,1)}, bf16[160,2048]{1,0:T(8,128)(2,1)}, u32[]{:S(2)}, u32[]{:S(2)}) collective-permute-start(bf16[160,2048]{1,0:T(8,128)(2,1)} %param.11), channel_id=1, source_target_pairs={{0,1},{1,2},{2,3},{3,0},{4,5},{5,6},{6,7},{7,4},{8,9},{9,10},{10,1... | collective-permute-start | bytes 1966088 | tf_op jit(solution)/shard_map/ppermute | solution.py:180
  8.8 20.6 %copy-start.1 = (bf16[640,1408]{1,0:T(8,128)(2,1)S(1)}, bf16[640,1408]{1,0:T(8,128)(2,1)}, u32[]{:S(2)}) copy-start(bf16[640,1408]{1,0:T(8,128)(2,1)} %fusion.16.hidden) | copy-start | bytes 5406724
  19.8 9.6 %collective-permute-start.24 = (bf16[80,2048]{1,0:T(8,128)(2,1)S(1)}, bf16[80,2048]{1,0:T(8,128)(2,1)S(1)}, u32[]{:S(2)}, u32[]{:S(2)}) collective-permute-start(bf16[80,2048]{1,0:T(8,128)(2,1)S(1)} %slice.98), channel_id=1, source_target_pairs={{0,1},{1,2},{2,3},{3,0},{4,5},{5,6},{6,7},{7,4},{8,9},{9,10},{10,1... | collective-permute-start | bytes 983048 | tf_op jit(solution)/shard_map/ppermute | solution.py:180
  20.3 9.1 %collective-permute-start.25 = (bf16[80,2048]{1,0:T(8,128)(2,1)S(1)}, bf16[80,2048]{1,0:T(8,128)(2,1)S(1)}, u32[]{:S(2)}, u32[]{:S(2)}) collective-permute-start(bf16[80,2048]{1,0:T(8,128)(2,1)S(1)} %slice.99), channel_id=1, source_target_pairs={{0,3},{1,0},{2,1},{3,2},{4,7},{5,4},{6,5},{7,6},{8,11},{9,8},{10,9... | collective-permute-start | bytes 983048 | tf_op jit(solution)/shard_map/ppermute | solution.py:180
  29.5 7.1 %copy-start.30 = (bf16[1408,32]{0,1:T(8,128)(2,1)S(1)}, bf16[1408,32]{0,1:T(8,128)(2,1)}, u32[]{:S(2)}) copy-start(bf16[1408,32]{0,1:T(8,128)(2,1)} %param.12) | copy-start | bytes 270340
  36.5 36.8 %collective-permute-start.26 = (bf16[4,8,32,1408]{3,2,1,0:T(8,128)(2,1)S(1)}, bf16[4,8,32,1408]{3,2,1,0:T(8,128)(2,1)S(1)}, u32[]{:S(2)}, u32[]{:S(2)}) collective-permute-start(bf16[4,8,32,1408]{3,2,1,0:T(8,128)(2,1)S(1)} %get-tuple-element.21), channel_id=1, source_target_pairs={{0,4},{4,0},{8,12},{12,8},{16,20},{20,16},{24,28},{28,24},{32,36},... | collective-permute-start | bytes 8650760 | tf_op jit(solution)/shard_map/ppermute | solution.py:176
  36.6 6.3 %collective-permute-start.2 = (bf16[32,1408]{1,0:T(8,128)(2,1)S(1)}, bf16[32,1408]{1,0:T(8,128)(2,1)S(1)}, u32[]{:S(2)}, u32[]{:S(2)}) collective-permute-start(bf16[32,1408]{1,0:T(8,128)(2,1)S(1)} %bitcast.82), channel_id=1, source_target_pairs={{0,8},{4,12},{8,16},{12,20},{16,24},{20,28},{24,0},{28,4},{32,40},... | collective-permute-start | bytes 270344 | tf_op jit(solution)/shard_map/ppermute | solution.py:176
  38.2 7.8 %collective-permute-start.1 = (bf16[32,1408]{1,0:T(8,128)(2,1)S(1)}, bf16[32,1408]{1,0:T(8,128)(2,1)S(1)}, u32[]{:S(2)}, u32[]{:S(2)}) collective-permute-start(bf16[32,1408]{1,0:T(8,128)(2,1)S(1)} %bitcast.83), channel_id=1, source_target_pairs={{0,16},{4,20},{8,24},{12,28},{16,0},{20,4},{24,8},{28,12},{32,48},... | collective-permute-start | bytes 270344 | tf_op jit(solution)/shard_map/ppermute | solution.py:176
  41.2 4.8 %collective-permute-start = (bf16[32,1408]{1,0:T(8,128)(2,1)S(1)}, bf16[32,1408]{1,0:T(8,128)(2,1)S(1)}, u32[]{:S(2)}, u32[]{:S(2)}) collective-permute-start(bf16[32,1408]{1,0:T(8,128)(2,1)S(1)} %bitcast.84), channel_id=1, source_target_pairs={{0,24},{4,28},{8,0},{12,4},{16,8},{20,12},{24,16},{28,20},{32,56},... | collective-permute-start | bytes 270344 | tf_op jit(solution)/shard_map/ppermute | solution.py:176
  46.1 13.3 %collective-permute-start.3 = (bf16[4,32,1408]{2,1,0:T(8,128)(2,1)S(1)}, bf16[4,32,1408]{2,1,0:T(8,128)(2,1)S(1)}, u32[]{:S(2)}, u32[]{:S(2)}) collective-permute-start(bf16[4,32,1408]{2,1,0:T(8,128)(2,1)S(1)} %pad_maximum_fusion.refs_0_), channel_id=1, source_target_pairs={{0,224},{4,228},{8,232},{12,236},{16,240},{20,244},{24,248},{28,25... | collective-permute-start | bytes 1081352 | tf_op jit(solution)/shard_map/ppermute | solution.py:176
  52.0 11.1 %collective-permute-start.6 = (bf16[4,32,1408]{2,1,0:T(8,128)(2,1)S(1)}, bf16[4,32,1408]{2,1,0:T(8,128)(2,1)S(1)}, u32[]{:S(2)}, u32[]{:S(2)}) collective-permute-start(bf16[4,32,1408]{2,1,0:T(8,128)(2,1)S(1)} %pad_maximum_fusion.refs_0_), channel_id=1, source_target_pairs={{0,32},{4,36},{8,40},{12,44},{16,48},{20,52},{24,56},{28,60},{32,6... | collective-permute-start | bytes 1081352 | tf_op jit(solution)/shard_map/ppermute | solution.py:176
  59.4 24.3 %copy-start.2 = (bf16[4,32,1408]{2,1,0:T(8,128)(2,1)}, bf16[4,32,1408]{2,1,0:T(8,128)(2,1)S(1)}, u32[]{:S(2)}) copy-start(bf16[4,32,1408]{2,1,0:T(8,128)(2,1)S(1)} %collective-permute-done.3.refs_1_) | copy-start | bytes 1081348
  59.4 10.2 %collective-permute-start.4 = (bf16[4,32,1408]{2,1,0:T(8,128)(2,1)S(1)}, bf16[4,32,1408]{2,1,0:T(8,128)(2,1)S(1)}, u32[]{:S(2)}, u32[]{:S(2)}) collective-permute-start(bf16[4,32,1408]{2,1,0:T(8,128)(2,1)S(1)} %collective-permute-done.3.refs_1_), channel_id=1, source_target_pairs={{0,224},{4,228},{8,232},{12,236},{16,240},{20,244},{24,248},{28,25... | collective-permute-start | bytes 1081352 | tf_op jit(solution)/shard_map/ppermute | solution.py:176
  63.1 32.7 %copy-start.4 = (bf16[4,32,1408]{2,1,0:T(8,128)(2,1)}, bf16[4,32,1408]{2,1,0:T(8,128)(2,1)S(1)}, u32[]{:S(2)}) copy-start(bf16[4,32,1408]{2,1,0:T(8,128)(2,1)S(1)} %collective-permute-done.6.refs_7_) | copy-start | bytes 1081348
  63.1 10.2 %collective-permute-start.7 = (bf16[4,32,1408]{2,1,0:T(8,128)(2,1)S(1)}, bf16[4,32,1408]{2,1,0:T(8,128)(2,1)S(1)}, u32[]{:S(2)}, u32[]{:S(2)}) collective-permute-start(bf16[4,32,1408]{2,1,0:T(8,128)(2,1)S(1)} %collective-permute-done.6.refs_7_), channel_id=1, source_target_pairs={{0,32},{4,36},{8,40},{12,44},{16,48},{20,52},{24,56},{28,60},{32,6... | collective-permute-start | bytes 1081352 | tf_op jit(solution)/shard_map/ppermute | solution.py:176
  69.6 26.8 %copy-start.6 = (bf16[4,32,1408]{2,1,0:T(8,128)(2,1)}, bf16[4,32,1408]{2,1,0:T(8,128)(2,1)S(1)}, u32[]{:S(2)}) copy-start(bf16[4,32,1408]{2,1,0:T(8,128)(2,1)S(1)} %collective-permute-done.4.refs_2_) | copy-start | bytes 1081348
  69.6 14.0 %collective-permute-start.5 = (bf16[4,32,1408]{2,1,0:T(8,128)(2,1)S(1)}, bf16[4,32,1408]{2,1,0:T(8,128)(2,1)S(1)}, u32[]{:S(2)}, u32[]{:S(2)}) collective-permute-start(bf16[4,32,1408]{2,1,0:T(8,128)(2,1)S(1)} %collective-permute-done.4.refs_2_), channel_id=1, source_target_pairs={{0,224},{4,228},{8,232},{12,236},{16,240},{20,244},{24,248},{28,25... | collective-permute-start | bytes 1081352 | tf_op jit(solution)/shard_map/ppermute | solution.py:176
  73.3 23.7 %copy-start.8 = (bf16[4,32,1408]{2,1,0:T(8,128)(2,1)}, bf16[4,32,1408]{2,1,0:T(8,128)(2,1)S(1)}, u32[]{:S(2)}) copy-start(bf16[4,32,1408]{2,1,0:T(8,128)(2,1)S(1)} %collective-permute-done.7.refs_6_) | copy-start | bytes 1081348
  73.3 9.2 %collective-permute-start.8 = (bf16[4,32,1408]{2,1,0:T(8,128)(2,1)S(1)}, bf16[4,32,1408]{2,1,0:T(8,128)(2,1)}, u32[]{:S(2)}, u32[]{:S(2)}) collective-permute-start(bf16[4,32,1408]{2,1,0:T(8,128)(2,1)S(1)} %collective-permute-done.7.refs_6_), channel_id=1, source_target_pairs={{0,32},{4,36},{8,40},{12,44},{16,48},{20,52},{24,56},{28,60},{32,6... | collective-permute-start | bytes 1081352 | tf_op jit(solution)/shard_map/ppermute | solution.py:176
  75.1 31.0 %copy-start.21 = (bf16[640,1408]{1,0:T(8,128)(2,1)S(1)}, bf16[640,1408]{1,0:T(8,128)(2,1)}, u32[]{:S(2)}) copy-start(bf16[640,1408]{1,0:T(8,128)(2,1)} %param.8) | copy-start | bytes 5406724
  75.1 31.0 %copy-start.22 = (bf16[640,1408]{1,0:T(8,128)(2,1)S(1)}, bf16[640,1408]{1,0:T(8,128)(2,1)}, u32[]{:S(2)}) copy-start(bf16[640,1408]{1,0:T(8,128)(2,1)} %param.7) | copy-start | bytes 5406724
  75.1 21.3 %collective-permute-start.28 = (bf16[8,32,1408]{2,1,0:T(8,128)(2,1)S(1)}, bf16[8,32,1408]{2,1,0:T(8,128)(2,1)S(1)}, u32[]{:S(2)}, u32[]{:S(2)}) collective-permute-start(bf16[8,32,1408]{2,1,0:T(8,128)(2,1)S(1)} %get-tuple-element.22), channel_id=1, source_target_pairs={{0,8},{4,12},{8,16},{12,20},{16,24},{20,28},{24,0},{28,4},{32,40},... | collective-permute-start | bytes 2162696 | tf_op jit(solution)/shard_map/ppermute | solution.py:176
  75.1 21.9 %collective-permute-start.27 = (bf16[8,32,1408]{2,1,0:T(8,128)(2,1)S(1)}, bf16[8,32,1408]{2,1,0:T(8,128)(2,1)S(1)}, u32[]{:S(2)}, u32[]{:S(2)}) collective-permute-start(bf16[8,32,1408]{2,1,0:T(8,128)(2,1)S(1)} %get-tuple-element.24), channel_id=1, source_target_pairs={{0,24},{4,28},{8,0},{12,4},{16,8},{20,12},{24,16},{28,20},{32,56},... | collective-permute-start | bytes 2162696 | tf_op jit(solution)/shard_map/ppermute | solution.py:176
  83.5 6.8 %collective-permute-start.9 = (bf16[2,32,1408]{2,1,0:T(8,128)(2,1)S(1)}, bf16[2,32,1408]{2,1,0:T(8,128)(2,1)S(1)}, u32[]{:S(2)}, u32[]{:S(2)}) collective-permute-start(bf16[2,32,1408]{2,1,0:T(8,128)(2,1)S(1)} %slice.96), channel_id=1, source_target_pairs={{0,32},{4,36},{8,40},{12,44},{16,48},{20,52},{24,56},{28,60},{32,6... | collective-permute-start | bytes 540680 | tf_op jit(solution)/shard_map/ppermute | solution.py:176
  83.5 14.6 %collective-permute-start.11 = (bf16[4,32,1408]{2,1,0:T(8,128)(2,1)S(1)}, bf16[4,32,1408]{2,1,0:T(8,128)(2,1)S(1)}, u32[]{:S(2)}, u32[]{:S(2)}) collective-permute-start(bf16[4,32,1408]{2,1,0:T(8,128)(2,1)S(1)} %pad_maximum_fusion.refs_0_), channel_id=1, source_target_pairs={{0,4},{4,0},{8,12},{12,8},{16,20},{20,16},{24,28},{28,24},{32,36},... | collective-permute-start | bytes 1081352 | tf_op jit(solution)/shard_map/ppermute | solution.py:176
  83.7 15.7 %collective-permute-start.12 = (bf16[4,32,1408]{2,1,0:T(8,128)(2,1)S(1)}, bf16[4,32,1408]{2,1,0:T(8,128)(2,1)S(1)}, u32[]{:S(2)}, u32[]{:S(2)}) collective-permute-start(bf16[4,32,1408]{2,1,0:T(8,128)(2,1)S(1)} %collective-permute-done.3.refs_1_), channel_id=1, source_target_pairs={{0,4},{4,0},{8,12},{12,8},{16,20},{20,16},{24,28},{28,24},{32,36},... | collective-permute-start | bytes 1081352 | tf_op jit(solution)/shard_map/ppermute | solution.py:176
  90.2 5.5 %collective-permute-start.10 = (bf16[2,32,1408]{2,1,0:T(8,128)(2,1)S(1)}, bf16[2,32,1408]{2,1,0:T(8,128)(2,1)S(1)}, u32[]{:S(2)}, u32[]{:S(2)}) collective-permute-start(bf16[2,32,1408]{2,1,0:T(8,128)(2,1)S(1)} %slice.97), channel_id=1, source_target_pairs={{0,224},{4,228},{8,232},{12,236},{16,240},{20,244},{24,248},{28,25... | collective-permute-start | bytes 540680 | tf_op jit(solution)/shard_map/ppermute | solution.py:176
  95.7 4.5 %collective-permute-start.18 = (bf16[4,32,1408]{2,1,0:T(8,128)(2,1)S(1)}, bf16[4,32,1408]{2,1,0:T(8,128)(2,1)S(1)}, u32[]{:S(2)}, u32[]{:S(2)}) collective-permute-start(bf16[4,32,1408]{2,1,0:T(8,128)(2,1)S(1)} %collective-permute-done.6.refs_7_), channel_id=1, source_target_pairs={{0,4},{4,0},{8,12},{12,8},{16,20},{20,16},{24,28},{28,24},{32,36},... | collective-permute-start | bytes 1081352 | tf_op jit(solution)/shard_map/ppermute | solution.py:176
  96.4 5.7 %copy-start.25 = (bf16[8,32,1408]{2,1,0:T(8,128)(2,1)}, bf16[8,32,1408]{2,1,0:T(8,128)(2,1)S(1)}, u32[]{:S(2)}) copy-start(bf16[8,32,1408]{2,1,0:T(8,128)(2,1)S(1)} %collective-permute-done.28) | copy-start | bytes 2162692
  96.4 5.0 %collective-permute-start.13 = (bf16[4,32,1408]{2,1,0:T(8,128)(2,1)S(1)}, bf16[4,32,1408]{2,1,0:T(8,128)(2,1)S(1)}, u32[]{:S(2)}, u32[]{:S(2)}) collective-permute-start(bf16[4,32,1408]{2,1,0:T(8,128)(2,1)S(1)} %collective-permute-done.4.refs_2_), channel_id=1, source_target_pairs={{0,4},{4,0},{8,12},{12,8},{16,20},{20,16},{24,28},{28,24},{32,36},... | collective-permute-start | bytes 1081352 | tf_op jit(solution)/shard_map/ppermute | solution.py:176
  97.0 5.9 %copy-start.27 = (bf16[8,32,1408]{2,1,0:T(8,128)(2,1)}, bf16[8,32,1408]{2,1,0:T(8,128)(2,1)S(1)}, u32[]{:S(2)}) copy-start(bf16[8,32,1408]{2,1,0:T(8,128)(2,1)S(1)} %collective-permute-done.27) | copy-start | bytes 2162692
  97.0 5.1 %collective-permute-start.17 = (bf16[4,32,1408]{2,1,0:T(8,128)(2,1)S(1)}, bf16[4,32,1408]{2,1,0:T(8,128)(2,1)S(1)}, u32[]{:S(2)}, u32[]{:S(2)}) collective-permute-start(bf16[4,32,1408]{2,1,0:T(8,128)(2,1)S(1)} %collective-permute-done.7.refs_6_), channel_id=1, source_target_pairs={{0,4},{4,0},{8,12},{12,8},{16,20},{20,16},{24,28},{28,24},{32,36},... | collective-permute-start | bytes 1081352 | tf_op jit(solution)/shard_map/ppermute | solution.py:176
  98.9 9.6 %collective-permute-start.14 = (bf16[4,32,1408]{2,1,0:T(8,128)(2,1)S(1)}, bf16[4,32,1408]{2,1,0:T(8,128)(2,1)}, u32[]{:S(2)}, u32[]{:S(2)}) collective-permute-start(bf16[4,32,1408]{2,1,0:T(8,128)(2,1)S(1)} %collective-permute-done.5.refs_3_), channel_id=1, source_target_pairs={{0,4},{4,0},{8,12},{12,8},{16,20},{20,16},{24,28},{28,24},{32,36},... | collective-permute-start | bytes 1081352 | tf_op jit(solution)/shard_map/ppermute | solution.py:176
  100.2 8.3 %collective-permute-start.16 = (bf16[4,32,1408]{2,1,0:T(8,128)(2,1)}, bf16[4,32,1408]{2,1,0:T(8,128)(2,1)}, u32[]{:S(2)}, u32[]{:S(2)}) collective-permute-start(bf16[4,32,1408]{2,1,0:T(8,128)(2,1)} %collective-permute-done.8.refs_5_), channel_id=1, source_target_pairs={{0,4},{4,0},{8,12},{12,8},{16,20},{20,16},{24,28},{28,24},{32,36},... | collective-permute-start | bytes 1081352 | tf_op jit(solution)/shard_map/ppermute | solution.py:176
  100.9 7.6 %collective-permute-start.15 = (bf16[4,32,1408]{2,1,0:T(8,128)(2,1)}, bf16[4,32,1408]{2,1,0:T(8,128)(2,1)}, u32[]{:S(2)}, u32[]{:S(2)}) collective-permute-start(bf16[4,32,1408]{2,1,0:T(8,128)(2,1)} %constant_dynamic-update-slice_fusion.refs_4_), channel_id=1, source_target_pairs={{0,4},{4,0},{8,12},{12,8},{16,20},{20,16},{24,28},{28,24},{32,36},... | collective-permute-start | bytes 1081352 | tf_op jit(solution)/shard_map/ppermute | solution.py:176
  102.1 38.3 %collective-permute-start.29 = (bf16[4,32,1408]{2,1,0:T(8,128)(2,1)}, bf16[4,32,1408]{2,1,0:T(8,128)(2,1)}, u32[]{:S(2)}, u32[]{:S(2)}) collective-permute-start(bf16[4,32,1408]{2,1,0:T(8,128)(2,1)} %get-tuple-element.30), channel_id=1, source_target_pairs={{0,8},{4,12},{8,16},{12,20},{16,24},{20,28},{24,0},{28,4},{32,40},... | collective-permute-start | bytes 1081352 | tf_op jit(solution)/shard_map/ppermute | solution.py:176
  102.9 37.6 %collective-permute-start.30 = (bf16[4,32,1408]{2,1,0:T(8,128)(2,1)}, bf16[4,32,1408]{2,1,0:T(8,128)(2,1)}, u32[]{:S(2)}, u32[]{:S(2)}) collective-permute-start(bf16[4,32,1408]{2,1,0:T(8,128)(2,1)} %get-tuple-element.31), channel_id=1, source_target_pairs={{0,24},{4,28},{8,0},{12,4},{16,8},{20,12},{24,16},{28,20},{32,56},... | collective-permute-start | bytes 1081352 | tf_op jit(solution)/shard_map/ppermute | solution.py:176
  108.5 1.5 copy-start
  110.0 1.0 copy-start.3
  111.0 1.0 copy-start.5
  112.0 1.0 copy-start.7
  112.9 1.0 copy-start.9
  113.9 1.0 copy-start.11
  114.9 1.0 copy-start.13
  115.9 1.0 copy-start.15
  116.9 1.0 copy-start.17
  117.9 1.0 copy-start.19
  118.9 21.6 %copy-start.20 = (f32[1,8,32,1408]{3,2,1,0:T(8,128)S(1)}, f32[1,8,32,1408]{3,2,1,0:T(8,128)}, u32[]{:S(2)}) copy-start(f32[1,8,32,1408]{3,2,1,0:T(8,128)} %get-tuple-element.25) | copy-start | bytes 4325380
  118.9 21.6 %copy-start.26 = (bf16[8,32,1408]{2,1,0:T(8,128)(2,1)S(1)}, bf16[8,32,1408]{2,1,0:T(8,128)(2,1)}, u32[]{:S(2)}) copy-start(bf16[8,32,1408]{2,1,0:T(8,128)(2,1)} %copy-done.25) | copy-start | bytes 2162692
  118.9 21.6 %copy-start.28 = (bf16[8,32,1408]{2,1,0:T(8,128)(2,1)S(1)}, bf16[8,32,1408]{2,1,0:T(8,128)(2,1)}, u32[]{:S(2)}) copy-start(bf16[8,32,1408]{2,1,0:T(8,128)(2,1)} %copy-done.27) | copy-start | bytes 2162692
  132.4 18.6 %collective-permute-start.21 = (bf16[160,2048]{1,0:T(8,128)(2,1)S(1)}, bf16[160,2048]{1,0:T(8,128)(2,1)S(1)}, u32[]{:S(2)}, u32[]{:S(2)}) collective-permute-start(bf16[160,2048]{1,0:T(8,128)(2,1)S(1)} %get-tuple-element.16), channel_id=1, source_target_pairs={{0,3},{1,0},{2,1},{3,2},{4,7},{5,4},{6,5},{7,6},{8,11},{9,8},{10,9... | collective-permute-start | bytes 1966088 | tf_op jit(solution)/shard_map/ppermute | solution.py:180
  135.4 18.6 %collective-permute-start.20 = (bf16[160,2048]{1,0:T(8,128)(2,1)S(1)}, bf16[160,2048]{1,0:T(8,128)(2,1)S(1)}, u32[]{:S(2)}, u32[]{:S(2)}) collective-permute-start(bf16[160,2048]{1,0:T(8,128)(2,1)S(1)} %get-tuple-element.15), channel_id=1, source_target_pairs={{0,1},{1,2},{2,3},{3,0},{4,5},{5,6},{6,7},{7,4},{8,9},{9,10},{10,1... | collective-permute-start | bytes 1966088 | tf_op jit(solution)/shard_map/ppermute | solution.py:180
  135.4 30.3 %collective-permute-start.19 = (bf16[160,2048]{1,0:T(8,128)(2,1)S(1)}, bf16[160,2048]{1,0:T(8,128)(2,1)S(1)}, u32[]{:S(2)}, u32[]{:S(2)}) collective-permute-start(bf16[160,2048]{1,0:T(8,128)(2,1)S(1)} %get-tuple-element.14), channel_id=1, source_target_pairs={{0,2},{1,3},{2,0},{3,1},{4,6},{5,7},{6,4},{7,5},{8,10},{9,11},{10,... | collective-permute-start | bytes 1966088 | tf_op jit(solution)/shard_map/ppermute | solution.py:180
  140.5 4.1 %copy-start.23 = (bf16[640,1408]{1,0:T(8,128)(2,1)S(1)}, bf16[640,1408]{1,0:T(8,128)(2,1)}, u32[]{:S(2)}) copy-start(bf16[640,1408]{1,0:T(8,128)(2,1)} %param.9) | copy-start | bytes 5406724
  140.5 4.1 %copy-start.24 = (bf16[640,1408]{1,0:T(8,128)(2,1)S(1)}, bf16[640,1408]{1,0:T(8,128)(2,1)}, u32[]{:S(2)}) copy-start(bf16[640,1408]{1,0:T(8,128)(2,1)} %param.10) | copy-start | bytes 5406724
  142.1 23.6 %collective-permute-start.37 = (bf16[32,1408]{1,0:T(8,128)(2,1)S(1)}, bf16[32,1408]{1,0:T(8,128)(2,1)S(1)}, u32[]{:S(2)}, u32[]{:S(2)}) collective-permute-start(bf16[32,1408]{1,0:T(8,128)(2,1)S(1)} %fusion.52), channel_id=1, source_target_pairs={{0,224},{4,228},{8,232},{12,236},{16,240},{20,244},{24,248},{28,25... | collective-permute-start | bytes 270344 | tf_op jit(solution)/shard_map/ppermute | solution.py:176
  143.7 25.8 %collective-permute-start.36 = (bf16[32,1408]{1,0:T(8,128)(2,1)S(1)}, bf16[32,1408]{1,0:T(8,128)(2,1)S(1)}, u32[]{:S(2)}, u32[]{:S(2)}) collective-permute-start(bf16[32,1408]{1,0:T(8,128)(2,1)S(1)} %get-tuple-element.37), channel_id=1, source_target_pairs={{0,32},{4,36},{8,40},{12,44},{16,48},{20,52},{24,56},{28,60},{32,6... | collective-permute-start | bytes 270344 | tf_op jit(solution)/shard_map/ppermute | solution.py:176
  151.0 29.4 %copy-start.29 = (f32[1408,32]{0,1:T(8,128)S(1)}, f32[1408,32]{0,1:T(8,128)}, u32[]{:S(2)}) copy-start(f32[1408,32]{0,1:T(8,128)} %param.13) | copy-start | bytes 540676
  151.0 21.8 %collective-permute-start.35 = (bf16[32,1408]{1,0:T(8,128)(2,1)S(1)}, bf16[32,1408]{1,0:T(8,128)(2,1)S(1)}, u32[]{:S(2)}, u32[]{:S(2)}) collective-permute-start(bf16[32,1408]{1,0:T(8,128)(2,1)S(1)} %get-tuple-element.36), channel_id=1, source_target_pairs={{0,192},{4,196},{8,200},{12,204},{16,208},{20,212},{24,216},{28,22... | collective-permute-start | bytes 270344 | tf_op jit(solution)/shard_map/ppermute | solution.py:176
  154.0 18.8 %collective-permute-start.34 = (bf16[32,1408]{1,0:T(8,128)(2,1)S(1)}, bf16[32,1408]{1,0:T(8,128)(2,1)S(1)}, u32[]{:S(2)}, u32[]{:S(2)}) collective-permute-start(bf16[32,1408]{1,0:T(8,128)(2,1)S(1)} %get-tuple-element.35), channel_id=1, source_target_pairs={{0,64},{4,68},{8,72},{12,76},{16,80},{20,84},{24,88},{28,92},{32,9... | collective-permute-start | bytes 270344 | tf_op jit(solution)/shard_map/ppermute | solution.py:176
  165.7 7.6 %collective-permute-start.33 = (bf16[32,1408]{1,0:T(8,128)(2,1)S(1)}, bf16[32,1408]{1,0:T(8,128)(2,1)S(1)}, u32[]{:S(2)}, u32[]{:S(2)}) collective-permute-start(bf16[32,1408]{1,0:T(8,128)(2,1)S(1)} %get-tuple-element.34), channel_id=1, source_target_pairs={{0,160},{4,164},{8,168},{12,172},{16,176},{20,180},{24,184},{28,18... | collective-permute-start | bytes 270344 | tf_op jit(solution)/shard_map/ppermute | solution.py:176
  165.7 11.1 %collective-permute-start.32 = (bf16[32,1408]{1,0:T(8,128)(2,1)S(1)}, bf16[32,1408]{1,0:T(8,128)(2,1)S(1)}, u32[]{:S(2)}, u32[]{:S(2)}) collective-permute-start(bf16[32,1408]{1,0:T(8,128)(2,1)S(1)} %get-tuple-element.33), channel_id=1, source_target_pairs={{0,96},{4,100},{8,104},{12,108},{16,112},{20,116},{24,120},{28,124... | collective-permute-start | bytes 270344 | tf_op jit(solution)/shard_map/ppermute | solution.py:176
  169.5 10.9 %collective-permute-start.31 = (bf16[32,1408]{1,0:T(8,128)(2,1)S(1)}, bf16[32,1408]{1,0:T(8,128)(2,1)S(1)}, u32[]{:S(2)}, u32[]{:S(2)}) collective-permute-start(bf16[32,1408]{1,0:T(8,128)(2,1)S(1)} %get-tuple-element.32), channel_id=1, source_target_pairs={{0,128},{4,132},{8,136},{12,140},{16,144},{20,148},{24,152},{28,15... | collective-permute-start | bytes 270344 | tf_op jit(solution)/shard_map/ppermute | solution.py:176
  (5 other events, 3.7 us)
